TPU v7x, 32 devices: a whole 2x2x4 slice. The times are simulated.
32 devices in a mesh: ep: 16 (over z, y, core), tp: 2 (over x).
Axes of the slice: x: 2, y: 2, z: 4, core: 2. Of those that a mesh axis runs over, the one named last changes fastest.
Arguments:
- tokens: bfloat16 [128, 1024], P('ep'), may hold values from -6 to 6
- ssm_state: float32 [128, 32, 64, 128], P('ep', 'tp'), may hold values from -6 to 6
- conv_x: bfloat16 [128, 3, 2048], P('ep', None, 'tp'), may hold values from -6 to 6
- conv_b: bfloat16 [128, 3, 1024], P('ep', None, 'tp'), may hold values from -6 to 6
- conv_c: bfloat16 [128, 3, 1024], P('ep', None, 'tp'), may hold values from -6 to 6
- w_x: bfloat16 [1024, 2048], P(None, 'tp'), may hold values from -0.1875 to 0.1875
- w_z: bfloat16 [1024, 2048], P(None, 'tp'), may hold values from -0.1875 to 0.1875
- w_b: bfloat16 [1024, 1024], P(None, 'tp'), may hold values from -0.1875 to 0.1875
- w_c: bfloat16 [1024, 1024], P(None, 'tp'), may hold values from -0.1875 to 0.1875
- w_dt: bfloat16 [1024, 32], replicated, may hold values from -0.1875 to 0.1875
- dt_bias: float32 [32], P('tp'), may hold values from -2 to 1
- a_log: float32 [32], P('tp'), may hold values from -3 to 1
- d_skip: float32 [32], P('tp'), may hold values from 0.1 to 1.9
- taps_x: bfloat16 [4, 2048], P(None, 'tp'), may hold values from -3 to 3
- taps_b: bfloat16 [4, 1024], P(None, 'tp'), may hold values from -3 to 3
- taps_c: bfloat16 [4, 1024], P(None, 'tp'), may hold values from -3 to 3
- norm1_gain: float32 [1024], replicated, may hold values from 0.1 to 1.9
- group_gain: float32 [2048], P('tp'), may hold values from 0.1 to 1.9
- w_out: bfloat16 [2048, 1024], P('tp'), may hold values from -0.125 to 0.125
- norm2_gain: float32 [1024], replicated, may hold values from 0.1 to 1.9
- route_ids: int32 [128, 6], P('ep'), may hold values from 0 to 15, all different within a row; in each aligned block of 8 rows (0 to 7, 8 to 15, ...) at most 6 rows name the same one
- route_weights: float32 [128, 6], P('ep'), may hold values from 0.1 to 1
- exp_gate: bfloat16 [16, 1024, 512], P('ep', None, 'tp'), may hold values from -0.1875 to 0.1875
- exp_up: bfloat16 [16, 1024, 512], P('ep', None, 'tp'), may hold values from -0.1875 to 0.1875
- exp_down: bfloat16 [16, 512, 1024], P('ep', 'tp'), may hold values from -0.25 to 0.25
- dense_gate: bfloat16 [1024, 1024], P('ep', 'tp'), may hold values from -0.1875 to 0.1875
- dense_up: bfloat16 [1024, 1024], P('ep', 'tp'), may hold values from -0.1875 to 0.1875
- dense_down: bfloat16 [1024, 1024], P('tp', 'ep'), may hold values from -0.1875 to 0.1875
- branch_gate: bfloat16 [1024], replicated, may hold values from -0.375 to 0.375
Outputs:
- mixed: bfloat16 [128, 1024], P('ep', 'tp')
- state_next: float32 [128, 32, 64, 128], P('ep', 'tp')
- conv_x_next: bfloat16 [128, 3, 2048], P('ep', None, 'tp')
- conv_b_next: bfloat16 [128, 3, 1024], P('ep', None, 'tp')
- conv_c_next: bfloat16 [128, 3, 1024], P('ep', None, 'tp')
Inputs may be any that keep to these rules, and one draw needn't show every extreme that they name: `route_ids`: each row names 6 different experts. Among the rows of one device no expert is named by more than 6 rows, a bound that some block reaches.
All inputs are finite; a program needn't handle non-finite values.
Results may differ from a plain program's by a relative error of at most 0.019.
Values may be sent and summed in bfloat16 or wider, within the bound.
A program may use at most 64 MiB of HBM per device.

v0:
```python
import jax
import jax.numpy as jnp
from jax import lax
from jax.sharding import PartitionSpec as P

epsilon = 1e-06


def rms_rows(values, gain):
    return values * lax.rsqrt(jnp.mean(values * values, axis=-1, keepdims=True) + epsilon) * gain


def short_conv(previous, fresh, taps):
    window = jnp.concatenate((previous, fresh[:, None]), axis=1)
    summed = jnp.sum(window.astype(jnp.float32) * taps.astype(jnp.float32)[None], axis=1)
    return (jax.nn.silu(summed), window[:, 1:])


def mixer_core(
    x_new,
    z_new,
    b_new,
    c_new,
    dt_raw,
    ssm_state,
    conv_x,
    conv_b,
    conv_c,
    dt_bias,
    a_log,
    d_skip,
    taps_x,
    taps_b,
    taps_c,
    group_gain,
):
    seqs, heads, head_dim, state_dim = ssm_state.shape
    groups = b_new.shape[1] // state_dim
    x_conv, conv_x_next = short_conv(conv_x, x_new, taps_x)
    b_conv, conv_b_next = short_conv(conv_b, b_new, taps_b)
    c_conv, conv_c_next = short_conv(conv_c, c_new, taps_c)
    x_heads = x_conv.reshape(seqs, heads, head_dim)
    b_heads = jnp.repeat(b_conv.reshape(seqs, groups, state_dim), heads // groups, axis=1)
    c_heads = jnp.repeat(c_conv.reshape(seqs, groups, state_dim), heads // groups, axis=1)
    step = jax.nn.softplus(dt_raw + dt_bias)
    decay = jnp.exp(-step * jnp.exp(a_log))
    state_next = (
        decay[:, :, None, None] * ssm_state
        + (step[:, :, None] * x_heads)[:, :, :, None] * b_heads[:, :, None, :]
    )
    readout = (
        jnp.einsum("shpn,shn->shp", state_next, c_heads, precision=lax.Precision.HIGHEST)
        + d_skip[None, :, None] * x_heads
    )
    gated = readout.reshape(seqs, heads * head_dim) * jax.nn.silu(z_new.astype(jnp.float32))
    grouped = gated.reshape(seqs, groups, -1)
    grouped = grouped * lax.rsqrt(jnp.mean(grouped * grouped, axis=-1, keepdims=True) + epsilon)
    mixed_heads = (grouped.reshape(seqs, heads * head_dim) * group_gain).astype(jnp.bfloat16)
    return (mixed_heads, state_next, conv_x_next, conv_b_next, conv_c_next)


def body(
    tokens,
    ssm_state,
    conv_x,
    conv_b,
    conv_c,
    w_x,
    w_z,
    w_b,
    w_c,
    w_dt,
    dt_bias,
    a_log,
    d_skip,
    taps_x,
    taps_b,
    taps_c,
    norm1_gain,
    group_gain,
    w_out,
    norm2_gain,
    route_ids,
    route_weights,
    exp_gate,
    exp_up,
    exp_down,
    dense_gate,
    dense_up,
    dense_down,
    branch_gate,
):
    seqs = tokens.shape[0]
    model_width = tokens.shape[1]
    stream = tokens.astype(jnp.float32)
    normed = rms_rows(stream, norm1_gain).astype(jnp.bfloat16)
    x_proj = jnp.dot(normed, w_x, preferred_element_type=jnp.float32).astype(jnp.bfloat16)
    z_proj = jnp.dot(normed, w_z, preferred_element_type=jnp.float32).astype(jnp.bfloat16)
    b_proj = jnp.dot(normed, w_b, preferred_element_type=jnp.float32).astype(jnp.bfloat16)
    c_proj = jnp.dot(normed, w_c, preferred_element_type=jnp.float32).astype(jnp.bfloat16)
    local_heads = ssm_state.shape[1]
    dt_columns = lax.dynamic_slice_in_dim(w_dt, lax.axis_index("tp") * local_heads, local_heads, 1)
    dt_raw = jnp.dot(normed, dt_columns, preferred_element_type=jnp.float32)
    mixed_heads, state_next, conv_x_next, conv_b_next, conv_c_next = mixer_core(
        x_proj,
        z_proj,
        b_proj,
        c_proj,
        dt_raw,
        ssm_state,
        conv_x,
        conv_b,
        conv_c,
        dt_bias,
        a_log,
        d_skip,
        taps_x,
        taps_b,
        taps_c,
        group_gain,
    )
    partial_out = jnp.dot(mixed_heads, w_out, preferred_element_type=jnp.float32)
    quarter = model_width // lax.axis_size("tp")
    column = lax.axis_index("tp") * quarter
    summed = lax.psum(partial_out.astype(jnp.bfloat16), "tp").astype(jnp.float32)
    residual = (stream + summed).astype(jnp.bfloat16)
    normed2 = rms_rows(residual.astype(jnp.float32), norm2_gain).astype(jnp.bfloat16)
    own_rows = lax.dynamic_slice_in_dim(residual, column, quarter, 1)
    experts_all = lax.axis_size("ep") * exp_gate.shape[0]
    top_count = route_ids.shape[1]
    capacity = min(seqs, max(2, 2 * seqs * top_count // experts_all))
    expert_iota = jnp.arange(experts_all, dtype=jnp.int32)
    matches = route_ids[:, :, None] == expert_iota[None, None, :]
    routed = jnp.sum(matches.astype(jnp.int32), axis=1)
    weight_of = jnp.sum(jnp.where(matches, route_weights[:, :, None], jnp.float32(0.0)), axis=1)
    ranked = jnp.cumsum(routed, axis=0) - routed
    slot_iota = jnp.arange(capacity, dtype=jnp.int32)
    slot_onehot = routed[:, :, None] * (ranked[:, :, None] == slot_iota[None, None, :]).astype(
        jnp.int32
    )
    dispatch = slot_onehot.reshape(seqs, experts_all * capacity).astype(jnp.bfloat16)
    outgoing = jnp.einsum(
        "sk,sd->kd", dispatch, normed2, preferred_element_type=jnp.float32
    ).astype(jnp.bfloat16)
    outgoing = outgoing.reshape(experts_all, capacity, model_width)
    arrived = lax.all_to_all(outgoing, "ep", split_axis=0, concat_axis=0, tiled=True)
    arrived_rows = arrived.reshape(-1, model_width)
    gate_pre = jnp.dot(arrived_rows, exp_gate[0], preferred_element_type=jnp.float32)
    up_pre = jnp.dot(arrived_rows, exp_up[0], preferred_element_type=jnp.float32)
    active = (jax.nn.silu(gate_pre) * up_pre).astype(jnp.bfloat16)
    expert_partial = jnp.dot(active, exp_down[0], preferred_element_type=jnp.float32)
    expert_part = lax.psum_scatter(
        expert_partial.astype(jnp.bfloat16), "tp", scatter_dimension=1, tiled=True
    )
    returned = lax.all_to_all(
        expert_part.reshape(-1, capacity, quarter), "ep", split_axis=0, concat_axis=0, tiled=True
    )
    combine = (weight_of[:, :, None] * slot_onehot.astype(jnp.float32)).reshape(
        seqs, experts_all * capacity
    )
    expert_sum = jnp.dot(
        combine,
        returned.reshape(experts_all * capacity, quarter).astype(jnp.float32),
        precision=lax.Precision.HIGHEST,
    )
    hidden_width = dense_gate.shape[1]
    spread = lax.all_to_all(normed2, "ep", split_axis=1, concat_axis=0, tiled=True)
    stacked = jnp.concatenate((dense_gate, dense_up), axis=1)
    joined = lax.psum_scatter(
        jnp.dot(spread, stacked, preferred_element_type=jnp.float32),
        "ep",
        scatter_dimension=0,
        tiled=True,
    )
    dense_active = (jax.nn.silu(joined[:, :hidden_width]) * joined[:, hidden_width:]).astype(
        jnp.bfloat16
    )
    every_active = lax.all_gather(dense_active, "ep", axis=0, tiled=True)
    column_part = jnp.dot(every_active, dense_down, preferred_element_type=jnp.float32).astype(
        jnp.bfloat16
    )
    dense_partial = lax.all_to_all(
        column_part, "ep", split_axis=0, concat_axis=1, tiled=True
    ).astype(jnp.float32)
    dense_out = lax.psum_scatter(
        dense_partial.astype(jnp.bfloat16), "tp", scatter_dimension=1, tiled=True
    ).astype(jnp.float32)
    branch = jax.nn.sigmoid(
        jnp.dot(normed2, branch_gate[:, None], preferred_element_type=jnp.float32)
    )
    mixed = (own_rows.astype(jnp.float32) + expert_sum + branch * dense_out).astype(jnp.bfloat16)
    return (mixed, state_next, conv_x_next, conv_b_next, conv_c_next)


def solution(mesh):
    return jax.shard_map(
        body,
        mesh=mesh,
        in_specs=(
            P("ep", None),
            P("ep", "tp", None, None),
            P("ep", None, "tp"),
            P("ep", None, "tp"),
            P("ep", None, "tp"),
            P(None, "tp"),
            P(None, "tp"),
            P(None, "tp"),
            P(None, "tp"),
            P(),
            P("tp"),
            P("tp"),
            P("tp"),
            P(None, "tp"),
            P(None, "tp"),
            P(None, "tp"),
            P(),
            P("tp"),
            P("tp", None),
            P(),
            P("ep", None),
            P("ep", None),
            P("ep", None, "tp"),
            P("ep", None, "tp"),
            P("ep", "tp", None),
            P("ep", "tp"),
            P("ep", "tp"),
            P("tp", "ep"),
            P(),
        ),
        out_specs=(
            P("ep", "tp"),
            P("ep", "tp", None, None),
            P("ep", None, "tp"),
            P("ep", None, "tp"),
            P("ep", None, "tp"),
        ),
        check_vma=False,
    )
```

profile of v0, /device:TPU:0, one launch (start us, length us, event | category | flops | bytes accessed | tf_op | source)
XLA Modules:
  0.0 177.8 jit_solution(14721564418474552331)
XLA Ops:
  7.3 1.0 fusion.32
  8.2 0.7 exp.43
  8.9 0.7 convert_element_type.98
  9.6 2.0 %fusion.2 = bf16[8,1,1024]{2,0,1:T(8,128)(2,1)S(1)} fusion(bf16[1024,1024]{1,0:T(8,128)(2,1)} %param.34, bf16[8,1024]{1,0:T(8,128)(2,1)} %param.29, f32[1024]{0:T(1024)} %param.45, f32[8]{0:T(128)S(1)} %add_rsqrt_fusion.2), kind=kOutput, calls=%fused_computation.10 | convolution fusion | flops 16818176 | bytes 2134048 | tf_op jit(solution)/shard_map/dot_general | solution.py:97
  11.7 0.8 multiply_reduce_fusion
  12.6 1.5 fusion.6
  14.1 0.7 convert_element_type.101
  14.8 0.7 multiply_reduce_fusion.2
  15.6 1.5 fusion.7
  17.3 0.2 multiply_exponential_fusion
  17.6 3.8 %multiply_add_fusion = f32[8,16,64,128]{3,2,1,0:T(8,128)S(1)} fusion(f32[8,16,64,128]{3,2,1,0:T(8,128)} %param.30, f32[8,16,128]{2,1,0:T(8,128)S(1)} %bitcast.75, f32[8,16,64]{2,1,0:T(8,128)S(1)} %broadcast_multiply_fusion, f32[8,16]{1,0:T(8,128)S(1)} %get-tuple-element.7), kind=kLoop, calls=%fused_computation | loop fusion | flops 3145728 | bytes 8487424 | tf_op jit(solution)/shard_map/add | solution.py:48
  21.4 2.0 %copy-done.1 = f32[8,16,64,128]{3,2,1,0:T(8,128)} copy-done((f32[8,16,64,128]{3,2,1,0:T(8,128)}, f32[8,16,64,128]{3,2,1,0:T(8,128)S(1)}, u32[]{:S(2)}) %copy-start.1) | copy-done | bytes 4194328
  23.4 6.6 %fusion.58 = f32[8,16,1,64]{3,2,1,0:T(1,128)S(1)} fusion(f32[8,16,64,128]{3,2,1,0:T(8,128)S(1)} %multiply_add_fusion, f32[8,16,128,1]{2,3,1,0:T(1,128)S(1)} %bitcast.76), kind=kOutput, calls=%fused_computation.99 | convolution fusion | flops 12582912 | bytes 4292608 | tf_op jit(solution)/shard_map/shpn,shn->shp/dot_general | solution.py:52
  30.2 0.4 fusion.56
  30.8 2.0 %convolution_convert_fusion.3 = bf16[8,1024]{1,0:T(8,128)(2,1)S(1)} fusion(bf16[1024,1024]{1,0:T(8,128)(2,1)} %param.47, f32[8,1024]{1,0:T(8,128)S(1)} %get-tuple-element.10, f32[8,1024]{1,0:T(8,128)S(1)} %bitcast.78, f32[1024]{0:T(1024)S(1)} %copy-done.11), kind=kOutput, calls=%fused_computation.6 | convolution fusion | flops 16809984 | bytes 2183168 | tf_op jit(solution)/shard_map/dot_general | solution.py:122
  32.8 9.8 %psum.7 = bf16[8,1024]{1,0:T(8,128)(2,1)S(1)} all-reduce(bf16[8,1024]{1,0:T(8,128)(2,1)S(1)} %convolution_convert_fusion.3), channel_id=1, replica_groups=mesh['ep'=16,'tp'=2] {'tp'}, use_global_device_ids=true, to_apply=%region_5.6 | all-reduce | flops 8192 | bytes 32768 | tf_op jit(solution)/shard_map/psum | solution.py:125
  42.6 0.1 fusion.29
  42.8 0.1 all_to_all.36
  43.0 0.7 reshape.127
  43.7 5.9 %all-to-all-start.2 = ((bf16[16,2,256]{2,1,0:T(2,128)(2,1)}), bf16[16,2,256]{2,1,0:T(2,128)(2,1)S(1)}, u32[]{:S(2)}, u32[]{:S(2)}) async-start(bf16[16,2,256]{2,1,0:T(2,128)(2,1)} %reshape.127), calls=%async_computation.3 | async-start | bytes 32768 | tf_op jit(solution)/shard_map/all_to_all | solution.py:167
  49.8 0.1 eq.43
  50.0 0.1 mul.250
  50.2 0.3 convolution_convert_fusion.1
  50.5 0.8 reshape.119
  51.3 4.7 %all-to-all-done.2 = bf16[16,2,256]{2,1,0:T(2,128)(2,1)S(1)} async-done(((bf16[16,2,256]{2,1,0:T(2,128)(2,1)}), bf16[16,2,256]{2,1,0:T(2,128)(2,1)S(1)}, u32[]{:S(2)}, u32[]{:S(2)}) %all-to-all-start.2) | async-done | bytes 16416 | tf_op jit(solution)/shard_map/all_to_all | solution.py:167
  56.1 3.5 %all-to-all-start = ((bf16[16,6,1024]{2,1,0:T(8,128)(2,1)}), bf16[16,6,1024]{2,1,0:T(8,128)(2,1)S(1)}, u32[]{:S(2)}, u32[]{:S(2)}) async-start(bf16[16,6,1024]{2,1,0:T(8,128)(2,1)} %reshape.119), calls=%async_computation | async-start | bytes 524288 | tf_op jit(solution)/shard_map/all_to_all | solution.py:146
  59.8 1.0 fusion.17
  60.9 0.1 convert_multiply_fusion
  61.1 8.5 %all-to-all-done = bf16[16,6,1024]{2,1,0:T(8,128)(2,1)S(1)} async-done(((bf16[16,6,1024]{2,1,0:T(8,128)(2,1)}), bf16[16,6,1024]{2,1,0:T(8,128)(2,1)S(1)}, u32[]{:S(2)}, u32[]{:S(2)}) %all-to-all-start) | async-done | bytes 196640 | tf_op jit(solution)/shard_map/all_to_all | solution.py:146
  69.6 1.3 fusion.15
  70.9 2.2 %convolution_convert_fusion = bf16[96,1024]{1,0:T(8,128)(2,1)} fusion(bf16[96,1024]{1,0:T(8,128)(2,1)S(1)} %reshape.120, bf16[1,256,1024]{2,1,0:T(8,128)(2,1)S(1)} %copy-done.3, bf16[1,1024,256]{2,1,0:T(8,128)(2,1)} %param.52, f32[96,256]{1,0:T(8,128)S(1)} %fusion.15), kind=kOutput, calls=%fused_computation.1 | convolution fusion | flops 100909056 | bytes 1540096 | tf_op jit(solution)/shard_map/dot_general | solution.py:151
  73.2 47.3 %reduce-scatter.6.cloned.1.call-done = f32[8,1024]{1,0:T(8,128)} async-done(((f32[128,1024]{1,0:T(8,128)}), f32[8,1024]{1,0:T(8,128)}) %reduce-scatter.6.cloned.1.call-update) | async-done | bytes 32784 | tf_op jit(solution)/shard_map/reduce_scatter | solution.py:169
  120.5 0.7 fusion.40
  121.3 19.8 %all_gather.3 = bf16[128,512]{1,0:T(8,128)(2,1)S(1)} all-gather(bf16[8,512]{1,0:T(8,128)(2,1)S(1)} %fusion.40), channel_id=1, replica_groups=mesh['ep'=16,'tp'=2] {'ep'}, dimensions={0}, use_global_device_ids=true | all-gather | bytes 139264 | tf_op jit(solution)/shard_map/all_gather | solution.py:178
  141.0 0.2 convolution_convert_fusion.2
  141.2 0.1 copy.51
  141.3 0.7 reshape.129
  142.0 3.5 %all-to-all-start.3 = ((bf16[16,2,256]{2,1,0:T(2,128)(2,1)}), bf16[16,2,256]{2,1,0:T(2,128)(2,1)S(1)}, u32[]{:S(2)}, u32[]{:S(2)}) async-start(bf16[16,2,256]{2,1,0:T(2,128)(2,1)} %reshape.129), calls=%async_computation.5 | async-start | bytes 32768 | tf_op jit(solution)/shard_map/all_to_all | solution.py:182
  145.5 0.1 fusion.11
  145.7 1.6 reshape.121
  147.2 4.7 %all-to-all-done.3 = bf16[16,2,256]{2,1,0:T(2,128)(2,1)S(1)} async-done(((bf16[16,2,256]{2,1,0:T(2,128)(2,1)}), bf16[16,2,256]{2,1,0:T(2,128)(2,1)S(1)}, u32[]{:S(2)}, u32[]{:S(2)}) %all-to-all-start.3) | async-done | bytes 16416 | tf_op jit(solution)/shard_map/all_to_all | solution.py:182
  152.0 3.5 %all-to-all-start.1 = ((bf16[16,6,512]{2,1,0:T(8,128)(2,1)}), bf16[16,6,512]{2,1,0:T(8,128)(2,1)S(1)}, u32[]{:S(2)}, u32[]{:S(2)}) async-start(bf16[16,6,512]{2,1,0:T(8,128)(2,1)} %reshape.121), calls=%async_computation.2 | async-start | bytes 262144 | tf_op jit(solution)/shard_map/all_to_all | solution.py:155
  155.6 0.6 fusion.38
  156.3 0.7 all_to_all.43
  157.1 0.6 fusion.27
  157.7 0.1 copy.48
  157.8 12.0 %reduce-scatter.8.cloned.1.call-done = bf16[8,512]{1,0:T(8,128)(2,1)} async-done(((bf16[8,1024]{1,0:T(8,128)(2,1)}), bf16[8,512]{1,0:T(8,128)(2,1)}) %reduce-scatter.8.cloned.1.call-update) | async-done | bytes 8208 | tf_op jit(solution)/shard_map/reduce_scatter | solution.py:185
  169.8 1.5 fusion.5
  (81 shorter events, 1.9 us)
Async XLA Ops:
  7.2 23.0 %copy-start = (bf16[1024,1024]{1,0:T(8,128)(2,1)S(1)}, bf16[1024,1024]{1,0:T(8,128)(2,1)}, u32[]{:S(2)}) copy-start(bf16[1024,1024]{1,0:T(8,128)(2,1)} %param.35) | copy-start | bytes 6291460
  7.2 10.0 %copy-start.2 = (bf16[8,1024]{1,0:T(8,128)(2,1)S(1)}, bf16[8,1024]{1,0:T(8,128)(2,1)}, u32[]{:S(2)}) copy-start(bf16[8,1024]{1,0:T(8,128)(2,1)} %param.29) | copy-start | bytes 49156
  7.2 10.0 %copy-start.7 = (f32[1024]{0:T(1024)S(1)}, f32[1024]{0:T(1024)}, u32[]{:S(2)}) copy-start(f32[1024]{0:T(1024)} %param.45) | copy-start | bytes 12292
  7.2 9.9 %copy-start.12 = (bf16[4,512]{1,0:T(4,128)(2,1)S(1)}, bf16[4,512]{1,0:T(4,128)(2,1)}, u32[]{:S(2)}) copy-start(bf16[4,512]{1,0:T(4,128)(2,1)} %param.44) | copy-start | bytes 12292
  7.2 9.9 %copy-start.6 = (bf16[8,3,512]{2,0,1:T(8,128)(2,1)S(1)}, bf16[8,3,512]{2,0,1:T(8,128)(2,1)}, u32[]{:S(2)}) copy-start(bf16[8,3,512]{2,0,1:T(8,128)(2,1)} %param.33) | copy-start | bytes 73732
  7.2 10.0 %copy-start.18 = (bf16[1024,32]{0,1:T(8,128)(2,1)S(1)}, bf16[1024,32]{0,1:T(8,128)(2,1)}, u32[]{:S(2)}) copy-start(bf16[1024,32]{0,1:T(8,128)(2,1)} %param.38) | copy-start | bytes 196612
  7.2 10.0 %copy-start.19 = (f32[16]{0:T(128)S(1)}, f32[16]{0:T(128)}, u32[]{:S(2)}) copy-start(f32[16]{0:T(128)} %param.39) | copy-start | bytes 196
  21.4 2.0 %copy-start.1 = (f32[8,16,64,128]{3,2,1,0:T(8,128)}, f32[8,16,64,128]{3,2,1,0:T(8,128)S(1)}, u32[]{:S(2)}) copy-start(f32[8,16,64,128]{3,2,1,0:T(8,128)S(1)} %multiply_add_fusion) | copy-start | bytes 12582916
  21.4 8.6 %copy-start.17 = (f32[16]{0:T(128)S(1)}, f32[16]{0:T(128)}, u32[]{:S(2)}) copy-start(f32[16]{0:T(128)} %param.41) | copy-start | bytes 196
  21.4 9.4 %copy-start.11 = (f32[1024]{0:T(1024)S(1)}, f32[1024]{0:T(1024)}, u32[]{:S(2)}) copy-start(f32[1024]{0:T(1024)} %param.46) | copy-start | bytes 12292
  23.4 19.4 %copy-start.13 = (f32[1024]{0:T(1024)S(1)}, f32[1024]{0:T(1024)}, u32[]{:S(2)}) copy-start(f32[1024]{0:T(1024)} %param.48) | copy-start | bytes 12292
  23.4 26.2 %copy-start.14 = (s32[8,6]{1,0:T(8,128)S(1)}, s32[8,6]{1,0:T(8,128)}, u32[]{:S(2)}) copy-start(s32[8,6]{1,0:T(8,128)} %param.49) | copy-start | bytes 580
  23.4 27.8 %copy-start.15 = (f32[8,6]{1,0:T(8,128)S(1)}, f32[8,6]{1,0:T(8,128)}, u32[]{:S(2)}) copy-start(f32[8,6]{1,0:T(8,128)} %param.50) | copy-start | bytes 580
  30.0 29.8 %copy-start.9 = (bf16[64,512]{1,0:T(8,128)(2,1)S(1)}, bf16[64,512]{1,0:T(8,128)(2,1)}, u32[]{:S(2)}) copy-start(bf16[64,512]{1,0:T(8,128)(2,1)} %param.55) | copy-start | bytes 196612
  30.0 29.8 %copy-start.10 = (bf16[64,512]{1,0:T(8,128)(2,1)S(1)}, bf16[64,512]{1,0:T(8,128)(2,1)}, u32[]{:S(2)}) copy-start(bf16[64,512]{1,0:T(8,128)(2,1)} %param.54) | copy-start | bytes 196612
  30.0 30.9 %copy-start.16 = (bf16[1024]{0:T(1024)(128)(2,1)S(1)}, bf16[1024]{0:T(1024)(128)(2,1)}, u32[]{:S(2)}) copy-start(bf16[1024]{0:T(1024)(128)(2,1)} %param.57) | copy-start | bytes 6148
  30.2 40.7 %copy-start.3 = (bf16[1,256,1024]{2,1,0:T(8,128)(2,1)S(1)}, bf16[1,256,1024]{2,1,0:T(8,128)(2,1)}, u32[]{:S(2)}) copy-start(bf16[1,256,1024]{2,1,0:T(8,128)(2,1)} %param.53) | copy-start | bytes 1572868
  30.8 110.2 %copy-start.8 = (bf16[512,64]{0,1:T(8,128)(2,1)S(1)}, bf16[512,64]{0,1:T(8,128)(2,1)}, u32[]{:S(2)}) copy-start(bf16[512,64]{0,1:T(8,128)(2,1)} %param.56) | copy-start | bytes 196612
  32.8 122.8 %copy-start.5 = (bf16[8,3,512]{2,0,1:T(8,128)(2,1)S(1)}, bf16[8,3,512]{2,0,1:T(8,128)(2,1)}, u32[]{:S(2)}) copy-start(bf16[8,3,512]{2,0,1:T(8,128)(2,1)} %param.32) | copy-start | bytes 73732
  32.8 124.2 %copy-start.4 = (bf16[8,3,1024]{2,0,1:T(8,128)(2,1)S(1)}, bf16[8,3,1024]{2,0,1:T(8,128)(2,1)}, u32[]{:S(2)}) copy-start(bf16[8,3,1024]{2,0,1:T(8,128)(2,1)} %param.31) | copy-start | bytes 147460
  43.7 12.4 %all-to-all-start.2 = ((bf16[16,2,256]{2,1,0:T(2,128)(2,1)}), bf16[16,2,256]{2,1,0:T(2,128)(2,1)S(1)}, u32[]{:S(2)}, u32[]{:S(2)}) async-start(bf16[16,2,256]{2,1,0:T(2,128)(2,1)} %reshape.127), calls=%async_computation.3 | async-start | bytes 32768 | tf_op jit(solution)/shard_map/all_to_all | solution.py:167
  56.1 13.5 %all-to-all-start = ((bf16[16,6,1024]{2,1,0:T(8,128)(2,1)}), bf16[16,6,1024]{2,1,0:T(8,128)(2,1)S(1)}, u32[]{:S(2)}, u32[]{:S(2)}) async-start(bf16[16,6,1024]{2,1,0:T(8,128)(2,1)} %reshape.119), calls=%async_computation | async-start | bytes 524288 | tf_op jit(solution)/shard_map/all_to_all | solution.py:146
  59.6 60.9 %reduce-scatter.6.cloned.1.call-start = ((), (), s32[]{:S(2)}) async-start(), calls=%async_computation.8 | async-start | bytes 557056 | tf_op jit(solution)/shard_map/reduce_scatter | solution.py:169
  60.8 84.9 %reduce-scatter.4.cloned.1.call-start = ((), (), s32[]{:S(2)}) async-start(), calls=%async_computation.7 | async-start | bytes 294912 | tf_op jit(solution)/shard_map/reduce_scatter | solution.py:152
  142.0 10.0 %all-to-all-start.3 = ((bf16[16,2,256]{2,1,0:T(2,128)(2,1)}), bf16[16,2,256]{2,1,0:T(2,128)(2,1)S(1)}, u32[]{:S(2)}, u32[]{:S(2)}) async-start(bf16[16,2,256]{2,1,0:T(2,128)(2,1)} %reshape.129), calls=%async_computation.5 | async-start | bytes 32768 | tf_op jit(solution)/shard_map/all_to_all | solution.py:182
  152.0 17.8 %all-to-all-start.1 = ((bf16[16,6,512]{2,1,0:T(8,128)(2,1)}), bf16[16,6,512]{2,1,0:T(8,128)(2,1)S(1)}, u32[]{:S(2)}, u32[]{:S(2)}) async-start(bf16[16,6,512]{2,1,0:T(8,128)(2,1)} %reshape.121), calls=%async_computation.2 | async-start | bytes 262144 | tf_op jit(solution)/shard_map/all_to_all | solution.py:155
  155.5 14.2 %reduce-scatter.8.cloned.1.call-start = ((), (), s32[]{:S(2)}) async-start(), calls=%async_computation.9 | async-start | bytes 24576 | tf_op jit(solution)/shard_map/reduce_scatter | solution.py:185
Sparse Core Ops, SparseCore 0:
  64.0 56.5 reduce-scatter.5
  122.7 10.0 reduce-scatter.3
  158.5 11.1 reduce-scatter.7
where the time goes:
time: 179 us; the launch traced here: 178 us
  waiting for transfers between devices  77.3 us (43%)
  blocking collectives  29.6 us (17%)
  matrix products  20.9 us (12%)
  starting transfers between devices  16.5 us (9%)
  between operations  14.2 us (8%)
  other arithmetic  10.6 us (6%)
  local copies, waits for them, and re-layouts  8.7 us (5%)
    reduce_scatter x1, waiting for transfers between devices, body(): lax.psum_scatter(jnp.dot(spread, stacked, preferred_element_type=jnp.floa...  47.3 us
    all_gather x1, blocking collectives, body(): every_active = lax.all_gather(dense_active, 'ep', axis=0, tiled=True)  19.8 us
    reduce_scatter x1, waiting for transfers between devices, body(): lax.psum_scatter(dense_partial.astype(jnp.bfloat16), 'tp', scatter_dimens...  12 us
    psum x1, blocking collectives, body(): lax.psum(partial_out.astype(jnp.bfloat16), 'tp').astype(jnp.float32)  9.81 us
    all_to_all x1, waiting for transfers between devices, body(): lax.all_to_all(outgoing, 'ep', split_axis=0, concat_axis=0, tiled=True)  8.5 us
    dot_general x1, matrix products, mixer_core(): jnp.einsum('shpn,shn->shp', state_next, c_heads, precision=lax.Precision....  6.58 us
    all_to_all x1, starting transfers between devices, body(): lax.all_to_all(normed2, 'ep', split_axis=1, concat_axis=0, tiled=True)  5.88 us
    all_to_all x1, waiting for transfers between devices, body(): lax.all_to_all(column_part, 'ep', split_axis=0, concat_axis=1, tiled=True)  4.75 us
  transfers between devices with their start and end apart: 7, of which 5 were waited for; matrix products, arithmetic and copies ran while one was open for 6% of the time, Pallas kernels for 0%

commit v1 on v0

v1 whole, which is shorter than its diff:
```python
import functools

import jax
import jax.numpy as jnp
from jax import lax
from jax.experimental import pallas as pl
from jax.experimental.pallas import tpu as pltpu
from jax.sharding import PartitionSpec as P

epsilon = 1e-06


def rms_rows(values, gain):
    return values * lax.rsqrt(jnp.mean(values * values, axis=-1, keepdims=True) + epsilon) * gain


def short_conv(previous, fresh, taps):
    window = jnp.concatenate((previous, fresh[:, None]), axis=1)
    summed = jnp.sum(window.astype(jnp.float32) * taps.astype(jnp.float32)[None], axis=1)
    return (jax.nn.silu(summed), window[:, 1:])


def mixer_core(
    x_new,
    z_new,
    b_new,
    c_new,
    dt_raw,
    ssm_state,
    conv_x,
    conv_b,
    conv_c,
    dt_bias,
    a_log,
    d_skip,
    taps_x,
    taps_b,
    taps_c,
    group_gain,
):
    seqs, heads, head_dim, state_dim = ssm_state.shape
    groups = b_new.shape[1] // state_dim
    x_conv, conv_x_next = short_conv(conv_x, x_new, taps_x)
    b_conv, conv_b_next = short_conv(conv_b, b_new, taps_b)
    c_conv, conv_c_next = short_conv(conv_c, c_new, taps_c)
    x_heads = x_conv.reshape(seqs, heads, head_dim)
    b_heads = jnp.repeat(b_conv.reshape(seqs, groups, state_dim), heads // groups, axis=1)
    c_heads = jnp.repeat(c_conv.reshape(seqs, groups, state_dim), heads // groups, axis=1)
    step = jax.nn.softplus(dt_raw + dt_bias)
    decay = jnp.exp(-step * jnp.exp(a_log))
    state_next = (
        decay[:, :, None, None] * ssm_state
        + (step[:, :, None] * x_heads)[:, :, :, None] * b_heads[:, :, None, :]
    )
    readout = (
        jnp.einsum("shpn,shn->shp", state_next, c_heads, precision=lax.Precision.HIGHEST)
        + d_skip[None, :, None] * x_heads
    )
    gated = readout.reshape(seqs, heads * head_dim) * jax.nn.silu(z_new.astype(jnp.float32))
    grouped = gated.reshape(seqs, groups, -1)
    grouped = grouped * lax.rsqrt(jnp.mean(grouped * grouped, axis=-1, keepdims=True) + epsilon)
    mixed_heads = (grouped.reshape(seqs, heads * head_dim) * group_gain).astype(jnp.bfloat16)
    return (mixed_heads, state_next, conv_x_next, conv_b_next, conv_c_next)


def tail_kernel(
    peers,
    splits,
    share,
    mixed_ref,
    w_out_hbm,
    tokens_ref,
    gain_ref,
    ids_ref,
    weights_ref,
    gate_hbm,
    up_hbm,
    down_hbm,
    stage_ref,
    branch_ref,
    out_ref,
    w_out,
    gate_up,
    down,
    partials,
    features,
    tables,
    dense,
    packed,
    returned,
    load_sem,
    part_send,
    part_recv,
    feat_send,
    feat_recv,
    table_send,
    table_recv,
    dense_send,
    dense_recv,
    ret_send,
    ret_recv,
):
    ep = lax.axis_index("ep")
    tp = lax.axis_index("tp")
    everyone = peers * splits
    me = ep * splits + tp
    seqs, width = tokens_ref.shape
    hidden = down.shape[0]
    part = width // splits

    loads = [
        pltpu.make_async_copy(w_out_hbm, w_out, load_sem.at[0]),
        pltpu.make_async_copy(gate_hbm.at[0], gate_up.at[:, pl.ds(0, hidden)], load_sem.at[1]),
        pltpu.make_async_copy(up_hbm.at[0], gate_up.at[:, pl.ds(hidden, hidden)], load_sem.at[2]),
        pltpu.make_async_copy(down_hbm.at[0], down, load_sem.at[3]),
    ]
    for load in loads:
        load.start()

    barrier = pltpu.get_barrier_semaphore()

    def greet(i, carry):
        other = lax.rem(me + i, everyone)
        pl.semaphore_signal(
            barrier,
            inc=1,
            device_id={"ep": other // splits, "tp": lax.rem(other, splits)},
            device_id_type=pl.DeviceIdType.MESH,
        )
        return carry

    lax.fori_loop(1, everyone, greet, 0)

    lanes = lax.broadcasted_iota(jnp.int32, tables.shape[1:], 1)
    table = jnp.zeros(tables.shape[1:], jnp.float32)
    for k in range(ids_ref.shape[1]):
        table = table + jnp.where(lanes == ids_ref[:, k : k + 1], weights_ref[:, k : k + 1], 0.0)
    tables[ep] = table
    dense[ep] = stage_ref[ep]

    loads[0].wait()
    partial_out = jnp.dot(mixed_ref[...], w_out[...], preferred_element_type=jnp.float32)
    partials[tp] = partial_out.astype(jnp.bfloat16)

    pl.semaphore_wait(barrier, everyone - 1)

    def part_copy(i, slot):
        return pltpu.make_async_remote_copy(
            src_ref=partials.at[slot],
            dst_ref=partials.at[slot],
            send_sem=part_send.at[i],
            recv_sem=part_recv.at[slot],
            device_id={"ep": ep, "tp": lax.rem(tp + i, splits)},
            device_id_type=pl.DeviceIdType.MESH,
        )

    def table_copy(i, slot):
        return pltpu.make_async_remote_copy(
            src_ref=tables.at[slot],
            dst_ref=tables.at[slot],
            send_sem=table_send.at[i],
            recv_sem=table_recv.at[slot],
            device_id={"ep": lax.rem(ep + i, peers), "tp": tp},
            device_id_type=pl.DeviceIdType.MESH,
        )

    def dense_copy(i, slot):
        return pltpu.make_async_remote_copy(
            src_ref=stage_ref.at[lax.rem(ep + i, peers)],
            dst_ref=dense.at[slot],
            send_sem=dense_send.at[i],
            recv_sem=dense_recv.at[slot],
            device_id={"ep": lax.rem(ep + i, peers), "tp": tp},
            device_id_type=pl.DeviceIdType.MESH,
        )

    def feat_copy(i, slot):
        return pltpu.make_async_remote_copy(
            src_ref=features.at[slot],
            dst_ref=features.at[slot],
            send_sem=feat_send.at[i],
            recv_sem=feat_recv.at[slot],
            device_id={"ep": lax.rem(ep + i, peers), "tp": tp},
            device_id_type=pl.DeviceIdType.MESH,
        )

    def ret_copy(i, slot):
        other = lax.rem(me + i, everyone)
        return pltpu.make_async_remote_copy(
            src_ref=packed.at[lax.rem(other, splits), other // splits],
            dst_ref=returned.at[slot],
            send_sem=ret_send.at[i],
            recv_sem=ret_recv.at[slot],
            device_id={"ep": other // splits, "tp": lax.rem(other, splits)},
            device_id_type=pl.DeviceIdType.MESH,
        )

    def start_all(copy, slot, count):
        def step(i, carry):
            copy(i, slot).start()
            return carry

        lax.fori_loop(1, count, step, 0)

    def take_all(copy, own, count):
        def step(i, carry):
            copy(i, lax.rem(own + count - i, count)).wait_recv()
            return carry

        lax.fori_loop(1, count, step, 0)

    def sent_all(copy, slot, count):
        def step(i, carry):
            copy(i, slot).wait_send()
            return carry

        lax.fori_loop(1, count, step, 0)

    start_all(part_copy, tp, splits)
    start_all(table_copy, ep, peers)
    start_all(dense_copy, ep, peers)

    take_all(part_copy, tp, splits)
    summed = partials[0].astype(jnp.float32)
    for t in range(1, splits):
        summed = summed + partials[t].astype(jnp.float32)
    residual = (tokens_ref[...].astype(jnp.float32) + summed).astype(jnp.bfloat16)
    residual = residual.astype(jnp.float32)
    normed2 = rms_rows(residual, gain_ref[...]).astype(jnp.bfloat16)
    features[ep] = normed2
    start_all(feat_copy, ep, peers)

    take_all(table_copy, ep, peers)
    take_all(dense_copy, ep, peers)
    every_table = tables[...].reshape(peers * seqs, tables.shape[2])
    columns = lax.broadcasted_iota(jnp.int32, every_table.shape, 1)
    own_weight = jnp.sum(jnp.where(columns == ep, every_table, 0.0), axis=1, keepdims=True)
    dense_weights = dense[...].reshape(width, dense.shape[2])
    for load in loads[1:]:
        load.wait()

    take_all(feat_copy, ep, peers)
    rows = features[...].astype(jnp.float32).reshape(peers * seqs, width)
    rows16 = rows.astype(jnp.bfloat16)
    pre = jnp.dot(rows16, gate_up[...], preferred_element_type=jnp.float32)
    active = own_weight * (jax.nn.silu(pre[:, :hidden]) * pre[:, hidden:])
    dense_pre = jnp.dot(rows16, dense_weights, preferred_element_type=jnp.float32)
    branch = jax.nn.sigmoid(
        jnp.sum(rows * branch_ref[...].astype(jnp.float32), axis=1, keepdims=True)
    )
    lane = lax.broadcasted_iota(jnp.int32, dense_pre.shape, 1)
    dense_act = jax.nn.silu(pltpu.roll(dense_pre, 2 * share, 1)) * pltpu.roll(dense_pre, share, 1)
    dense_act = jnp.where((lane >= 2 * share) & (lane < 3 * share), branch * dense_act, 0.0)
    total = jnp.dot(active.astype(jnp.bfloat16), down[...], preferred_element_type=jnp.float32)
    total = total + lax.dot_general(
        dense_act.astype(jnp.bfloat16),
        dense_weights,
        (((1,), (1,)), ((), ())),
        preferred_element_type=jnp.float32,
    )
    for t in range(splits):
        packed[t] = (
            total[:, t * part : (t + 1) * part].reshape(peers, seqs, part).astype(jnp.bfloat16)
        )
    returned[me] = packed[tp, ep]
    start_all(ret_copy, me, everyone)

    sent_all(part_copy, tp, splits)
    sent_all(table_copy, ep, peers)
    sent_all(dense_copy, ep, peers)
    sent_all(feat_copy, ep, peers)
    own_rows = residual[:, :part]
    for t in range(1, splits):
        own_rows = jnp.where(tp == t, residual[:, t * part : (t + 1) * part], own_rows)

    take_all(ret_copy, me, everyone)
    mixed = own_rows + jnp.sum(returned[...].astype(jnp.float32), axis=0)
    out_ref[...] = mixed.astype(jnp.bfloat16)
    sent_all(ret_copy, me, everyone)


def after_mixer(
    mixed_heads,
    w_out,
    tokens,
    norm2_gain,
    route_ids,
    route_weights,
    exp_gate,
    exp_up,
    exp_down,
    dense_gate,
    dense_up,
    dense_down,
    branch_gate,
):
    peers = lax.axis_size("ep")
    splits = lax.axis_size("tp")
    seqs, width = tokens.shape
    depth, local_hidden = dense_gate.shape
    share = local_hidden // peers
    hidden = exp_gate.shape[2]
    part = width // splits
    lanes = -(-3 * share // 128) * 128
    by_owner = lambda w: w.reshape(depth, peers, share).transpose(1, 0, 2)
    stage = jnp.concatenate(
        (
            by_owner(dense_gate),
            by_owner(dense_up),
            dense_down.reshape(peers, share, depth).transpose(0, 2, 1),
            jnp.zeros((peers, depth, lanes - 3 * share), jnp.bfloat16),
        ),
        axis=2,
    )
    vmem = pl.BlockSpec(memory_space=pltpu.VMEM)
    hbm = pl.BlockSpec(memory_space=pl.ANY)
    dma = lambda count: pltpu.SemaphoreType.DMA((count,))
    return pl.pallas_call(
        functools.partial(tail_kernel, peers, splits, share),
        out_shape=jax.ShapeDtypeStruct((seqs, part), jnp.bfloat16),
        in_specs=[vmem, hbm, vmem, vmem, vmem, vmem, hbm, hbm, hbm, vmem, vmem],
        out_specs=vmem,
        scratch_shapes=[
            pltpu.VMEM(w_out.shape, jnp.bfloat16),
            pltpu.VMEM((width, 2 * hidden), jnp.bfloat16),
            pltpu.VMEM((hidden, width), jnp.bfloat16),
            pltpu.VMEM((splits, seqs, width), jnp.bfloat16),
            pltpu.VMEM((peers, seqs, width), jnp.bfloat16),
            pltpu.VMEM((peers, seqs, 128), jnp.float32),
            pltpu.VMEM((peers, depth, lanes), jnp.bfloat16),
            pltpu.VMEM((splits, peers, seqs, part), jnp.bfloat16),
            pltpu.VMEM((peers * splits, seqs, part), jnp.bfloat16),
            dma(4),
            dma(splits),
            dma(splits),
            dma(peers),
            dma(peers),
            dma(peers),
            dma(peers),
            dma(peers),
            dma(peers),
            dma(peers * splits),
            dma(peers * splits),
        ],
        compiler_params=pltpu.CompilerParams(
            collective_id=0, has_side_effects=True, vmem_limit_bytes=32 * 1024 * 1024
        ),
        cost_estimate=pl.CostEstimate(flops=10**9, bytes_accessed=10**7, transcendentals=0),
    )(
        mixed_heads,
        w_out,
        tokens,
        norm2_gain[None],
        route_ids,
        route_weights,
        exp_gate,
        exp_up,
        exp_down,
        stage,
        branch_gate[None],
    )


def body(
    tokens,
    ssm_state,
    conv_x,
    conv_b,
    conv_c,
    w_x,
    w_z,
    w_b,
    w_c,
    w_dt,
    dt_bias,
    a_log,
    d_skip,
    taps_x,
    taps_b,
    taps_c,
    norm1_gain,
    group_gain,
    w_out,
    norm2_gain,
    route_ids,
    route_weights,
    exp_gate,
    exp_up,
    exp_down,
    dense_gate,
    dense_up,
    dense_down,
    branch_gate,
):
    stream = tokens.astype(jnp.float32)
    normed = rms_rows(stream, norm1_gain).astype(jnp.bfloat16)
    x_proj = jnp.dot(normed, w_x, preferred_element_type=jnp.float32).astype(jnp.bfloat16)
    z_proj = jnp.dot(normed, w_z, preferred_element_type=jnp.float32).astype(jnp.bfloat16)
    b_proj = jnp.dot(normed, w_b, preferred_element_type=jnp.float32).astype(jnp.bfloat16)
    c_proj = jnp.dot(normed, w_c, preferred_element_type=jnp.float32).astype(jnp.bfloat16)
    local_heads = ssm_state.shape[1]
    dt_columns = lax.dynamic_slice_in_dim(w_dt, lax.axis_index("tp") * local_heads, local_heads, 1)
    dt_raw = jnp.dot(normed, dt_columns, preferred_element_type=jnp.float32)
    mixed_heads, state_next, conv_x_next, conv_b_next, conv_c_next = mixer_core(
        x_proj,
        z_proj,
        b_proj,
        c_proj,
        dt_raw,
        ssm_state,
        conv_x,
        conv_b,
        conv_c,
        dt_bias,
        a_log,
        d_skip,
        taps_x,
        taps_b,
        taps_c,
        group_gain,
    )
    mixed = after_mixer(
        mixed_heads,
        w_out,
        tokens,
        norm2_gain,
        route_ids,
        route_weights,
        exp_gate,
        exp_up,
        exp_down,
        dense_gate,
        dense_up,
        dense_down,
        branch_gate,
    )
    return (mixed, state_next, conv_x_next, conv_b_next, conv_c_next)


def solution(mesh):
    return jax.shard_map(
        body,
        mesh=mesh,
        in_specs=(
            P("ep", None),
            P("ep", "tp", None, None),
            P("ep", None, "tp"),
            P("ep", None, "tp"),
            P("ep", None, "tp"),
            P(None, "tp"),
            P(None, "tp"),
            P(None, "tp"),
            P(None, "tp"),
            P(),
            P("tp"),
            P("tp"),
            P("tp"),
            P(None, "tp"),
            P(None, "tp"),
            P(None, "tp"),
            P(),
            P("tp"),
            P("tp", None),
            P(),
            P("ep", None),
            P("ep", None),
            P("ep", None, "tp"),
            P("ep", None, "tp"),
            P("ep", "tp", None),
            P("ep", "tp"),
            P("ep", "tp"),
            P("tp", "ep"),
            P(),
        ),
        out_specs=(
            P("ep", "tp"),
            P("ep", "tp", None, None),
            P("ep", None, "tp"),
            P("ep", None, "tp"),
            P("ep", None, "tp"),
        ),
        check_vma=False,
    )
```

time: 179 us -> 63.8 us (0.36)
  waiting for transfers between devices: 77.3 us -> 0 us
  blocking collectives: 29.6 us -> 0 us
  Pallas kernels: 0 us -> 29.3 us
  starting transfers between devices: 16.5 us -> 0 us
  between operations: 14.2 us -> 1.01 us
  matrix products: 20.9 us -> 13.1 us
    reduce_scatter x3 -> x0, waiting for transfers between devices: 59.3 us -> none  [the longest x1 47.3 us: body(): lax.psum_scatter(jnp.dot(spread, stacked, preferred_element_type=jnp.floa...]
    pallas_call x0 -> x1, Pallas kernels: none -> 29.3 us  [after_mixer(): pl.pallas_call(functools.partial(tail_kernel, peers, splits, share), out_...]
    all_gather x1 -> x0, blocking collectives: 19.8 us -> none  [body(): every_active = lax.all_gather(dense_active, 'ep', axis=0, tiled=True)]
    all_to_all x4 -> x0, waiting for transfers between devices: 18 us -> none  [the longest x1 8.5 us: body(): lax.all_to_all(outgoing, 'ep', split_axis=0, concat_axis=0, tiled=True)]
    all_to_all x4 -> x0, starting transfers between devices: 16.4 us -> none  [the longest x1 5.88 us: body(): lax.all_to_all(normed2, 'ep', split_axis=1, concat_axis=0, tiled=True)]
    psum x1 -> x0, blocking collectives: 9.81 us -> none  [body(): lax.psum(partial_out.astype(jnp.bfloat16), 'tp').astype(jnp.float32)]
    dot_general x8 -> x0, matrix products: 8.6 us -> none  [the longest x1 2.23 us: body(): jnp.dot(active, exp_down[0], preferred_element_type=jnp.float32)]
    reshape x3, local copies, waits for them, and re-layouts: 2.42 us -> 0.55 us  [the longest x2 0.36 us: after_mixer(): by_owner = lambda w: w.reshape(depth, peers, share).transpose(1, 0, 2)]
  transfers between devices with their start and end apart: 7 -> 0, of which waited for: 5 -> 0; matrix products, arithmetic and copies ran while one was open for 6% -> 0% of each run, Pallas kernels for 0% -> 0%
where the time goes in v1:
time: 63.8 us; the launch traced here: 63.1 us
  Pallas kernels  29.3 us (46%)
  matrix products  13.1 us (21%)
  other arithmetic  10 us (16%)
  local copies, waits for them, and re-layouts  9.54 us (15%)
  between operations  1.01 us (2%)
    pallas_call x1, Pallas kernels, after_mixer(): pl.pallas_call(functools.partial(tail_kernel, peers, splits, share), out_...  29.3 us
    dot_general x1, matrix products, mixer_core(): jnp.einsum('shpn,shn->shp', state_next, c_heads, precision=lax.Precision....  6.58 us
    unnamed x46, local copies, waits for them, and re-layouts  5.69 us
    add x1, other arithmetic, mixer_core(): decay[:, :, None, None] * ssm_state  3.82 us
    dot_general x1, matrix products, body(): jnp.dot(normed, w_x, preferred_element_type=jnp.float32)  2.04 us
    dot_general x1, matrix products, body(): jnp.dot(normed, w_b, preferred_element_type=jnp.float32)  1.55 us
    dot_general x1, matrix products, body(): jnp.dot(normed, w_c, preferred_element_type=jnp.float32)  1.54 us
    reduce_sum x3, other arithmetic, short_conv(): jnp.sum(window.astype(jnp.float32) * taps.astype(jnp.float32)[None], axis=1)  1.52 us

profile of v1, /device:TPU:0, one launch (start us, length us, event | category | flops | bytes accessed | tf_op | source)
XLA Modules:
  0.0 63.1 jit_solution(1982433857788472061)
XLA Ops:
  0.6 0.0 copy-start
  0.6 0.0 copy-start.13
  0.7 0.0 copy-start.12
  0.7 0.0 copy-start.11
  0.7 0.8 %exp.32 = f32[16]{0:T(128)S(1)} exponential(f32[16]{0:T(128)} %param.40) | non-fusion elementwise | bytes 128 | tf_op jit(solution)/shard_map/exp | solution.py:50
  1.5 0.8 %fusion.5 = f32[8]{0:T(128)S(1)} fusion(bf16[8,1024]{1,0:T(8,128)(2,1)} %tokens_ref.1), kind=kLoop, calls=%fused_computation.28 | loop fusion | flops 24568 | bytes 16416 | tf_op jit(solution)/shard_map/reduce_sum | solution.py:14
  2.4 0.1 pad.3.clone
  2.5 0.7 %broadcast_in_dim.44.branch_ref = bf16[1,1024]{1,0:T(2,128)(2,1)S(1)} reshape(bf16[1024]{0:T(1024)(128)(2,1)} %param.57) | data formatting | bytes 4096 | tf_op jit(solution)/shard_map/broadcast_in_dim | solution.py:360
  3.2 1.0 %multiply_exponential_fusion = (f32[8,16]{1,0:T(8,128)S(1)}, f32[8,16]{1,0:T(8,128)S(1)}) fusion(f32[16]{0:T(128)S(1)} %exp.32, f32[16]{0:T(128)} %param.39, bf16[1024,32]{0,1:T(8,128)(2,1)} %param.38, s32[]{:T(128)S(6)} %select_n.7, bf16[8,1024]{1,0:T(8,128)(2,1)} %tokens_ref.1, f32[1024]{0:T(1024)} %param.45, f32[8]{0:T(128)S(1)} %add_rsqrt_fusion.1), kind=kOutput, calls=%fused_computation.40 | convolution fusion | flops 296064 | bytes 54884 | tf_op jit(solution)/shard_map/dot_general | solution.py:403
  4.2 1.5 %fusion.2 = bf16[8,1,512]{2,0,1:T(8,128)(2,1)S(1)} fusion(bf16[1024,512]{1,0:T(8,128)(2,1)} %param.36, bf16[8,1024]{1,0:T(8,128)(2,1)} %tokens_ref.1, f32[1024]{0:T(1024)} %param.45, f32[8]{0:T(128)S(1)} %add_rsqrt_fusion.1), kind=kOutput, calls=%fused_computation.7 | convolution fusion | flops 8425472 | bytes 1077280 | tf_op jit(solution)/shard_map/dot_general | solution.py:399
  5.7 1.5 %fusion.3 = bf16[8,1,512]{2,0,1:T(8,128)(2,1)S(1)} fusion(bf16[1024,512]{1,0:T(8,128)(2,1)} %param.37, bf16[8,1024]{1,0:T(8,128)(2,1)} %tokens_ref.1, f32[1024]{0:T(1024)} %param.45, f32[8]{0:T(128)S(1)} %add_rsqrt_fusion.1), kind=kOutput, calls=%fused_computation.8 | convolution fusion | flops 8425472 | bytes 1077280 | tf_op jit(solution)/shard_map/dot_general | solution.py:400
  7.3 0.7 %convert_element_type.49 = f32[4,512]{1,0:T(4,128)S(1)} convert(bf16[4,512]{1,0:T(4,128)(2,1)} %param.43) | non-fusion elementwise | flops 2048 | bytes 12288 | tf_op jit(solution)/shard_map/convert_element_type | solution.py:19
  8.0 0.8 %multiply_reduce_fusion.2 = f32[8,512]{1,0:T(8,128)S(1)} fusion(bf16[8,1,512]{2,0,1:T(8,128)(2,1)S(1)} %fusion.2, bf16[8,3,512]{2,0,1:T(8,128)(2,1)} %param.32, f32[4,512]{1,0:T(4,128)S(1)} %convert_element_type.49), kind=kLoop, calls=%fused_computation.17 | loop fusion | flops 61440 | bytes 57344 | tf_op jit(solution)/shard_map/reduce_sum | solution.py:19
  8.7 0.7 %convert_element_type.52 = f32[4,512]{1,0:T(4,128)S(1)} convert(bf16[4,512]{1,0:T(4,128)(2,1)} %param.44) | non-fusion elementwise | flops 2048 | bytes 12288 | tf_op jit(solution)/shard_map/convert_element_type | solution.py:19
  9.4 0.8 %multiply_reduce_fusion.1 = f32[8,512]{1,0:T(8,128)S(1)} fusion(bf16[8,1,512]{2,0,1:T(8,128)(2,1)S(1)} %fusion.3, bf16[8,3,512]{2,0,1:T(8,128)(2,1)} %param.33, f32[4,512]{1,0:T(4,128)S(1)} %convert_element_type.52), kind=kLoop, calls=%fused_computation.16 | loop fusion | flops 61440 | bytes 57344 | tf_op jit(solution)/shard_map/reduce_sum | solution.py:19
  10.2 2.0 %fusion.1 = bf16[8,1,1024]{2,0,1:T(8,128)(2,1)S(1)} fusion(bf16[1024,1024]{1,0:T(8,128)(2,1)} %param.34, bf16[8,1024]{1,0:T(8,128)(2,1)} %tokens_ref.1, f32[1024]{0:T(1024)} %param.45, f32[8]{0:T(128)S(1)} %add_rsqrt_fusion.1), kind=kOutput, calls=%fused_computation.4 | convolution fusion | flops 16818176 | bytes 2134048 | tf_op jit(solution)/shard_map/dot_general | solution.py:397
  12.3 0.1 reduce_sum.53
  12.4 0.6 fusion.4
  13.0 0.6 fusion.9
  13.7 0.6 broadcast_in_dim.20
  14.3 0.1 broadcast_multiply_fusion
  14.4 0.1 copy.34
  14.5 0.2 copy.35
  14.7 0.1 copy.36
  14.8 0.2 copy.37
  15.0 0.1 copy.38
  15.2 0.2 copy.39
  15.4 0.3 maximum_maximum_fusion.stage_ref
  15.6 3.8 %multiply_add_fusion = f32[8,16,64,128]{3,2,1,0:T(8,128)S(1)} fusion(f32[8,16,64,128]{3,2,1,0:T(8,128)} %param.30, f32[8,16,128]{2,1,0:T(8,128)S(1)} %bitcast.38, f32[8,16,64]{2,1,0:T(8,128)S(1)} %broadcast_multiply_fusion, f32[8,16]{1,0:T(8,128)S(1)} %get-tuple-element.5), kind=kLoop, calls=%fused_computation | loop fusion | flops 3145728 | bytes 8487424 | tf_op jit(solution)/shard_map/add | solution.py:52
  19.5 0.0 copy-start.9
  19.5 2.0 %copy-done.9 = f32[8,16,64,128]{3,2,1,0:T(8,128)} copy-done((f32[8,16,64,128]{3,2,1,0:T(8,128)}, f32[8,16,64,128]{3,2,1,0:T(8,128)S(1)}, u32[]{:S(2)}) %copy-start.9) | copy-done | bytes 4194328
  21.5 0.0 copy-start.19
  21.5 0.0 copy-start.3
  21.5 0.0 copy-start.4
  21.5 0.0 copy-start.6
  21.5 0.0 copy-start.7
  21.6 0.0 copy-start.8
  21.6 6.6 %fusion.20 = f32[8,16,1,64]{3,2,1,0:T(1,128)S(1)} fusion(f32[8,16,64,128]{3,2,1,0:T(8,128)S(1)} %multiply_add_fusion, f32[8,16,128,1]{2,3,1,0:T(1,128)S(1)} %bitcast.37), kind=kOutput, calls=%fused_computation.45 | convolution fusion | flops 12582912 | bytes 4292608 | tf_op jit(solution)/shard_map/shpn,shn->shp/dot_general | solution.py:56
  28.2 0.7 %multiply_add_fusion.1 = f32[8,16,64]{2,1,0:T(8,128)} fusion(f32[8,16,64]{2,1,0:T(8,128)S(1)} %bitcast.36, f32[16]{0:T(128)S(1)} %copy-done.20, f32[8,16,64]{2,1,0:T(8,128)S(1)} %reduce_sum.53), kind=kLoop, calls=%fused_computation.15 | loop fusion | flops 49152 | bytes 98368 | tf_op jit(solution)/shard_map/add | solution.py:56
  28.9 0.9 %reshape.76 = f32[8,1024]{1,0:T(8,128)S(1)} reshape(f32[8,16,64]{2,1,0:T(8,128)} %multiply_add_fusion.1) | data formatting | bytes 65536 | tf_op jit(solution)/shard_map/reshape | solution.py:59
  29.8 0.4 fusion.19
  30.2 0.1 reduce_sum.58
  30.3 0.1 mul.177
  30.5 0.0 copy-start.1
  30.5 1.6 %copy-done.1 = bf16[1024,1024]{1,0:T(8,128)(2,1)S(1)} copy-done((bf16[1024,1024]{1,0:T(8,128)(2,1)S(1)}, bf16[1024,1024]{1,0:T(8,128)(2,1)}, u32[]{:S(2)}) %copy-start.1) | copy-done | bytes 2097176
  32.1 1.0 %copy-done.5 = bf16[1,256,1024]{2,1,0:T(8,128)(2,1)S(1)} copy-done((bf16[1,256,1024]{2,1,0:T(8,128)(2,1)S(1)}, bf16[1,256,1024]{2,1,0:T(8,128)(2,1)}, u32[]{:S(2)}) %copy-start.5) | copy-done | bytes 524312
  33.1 29.3 %shard_map.308 = bf16[8,512]{1,0:T(8,128)(2,1)S(1)} custom-call(bf16[8,1024]{1,0:T(8,128)(2,1)S(1)} %multiply_convert_fusion.mixed_ref, bf16[1024,1024]{1,0:T(8,128)(2,1)S(1)} %copy-done.1, bf16[8,1024]{1,0:T(8,128)(2,1)S(1)} %copy-done.2, f32[1,1024]{1,0:T(1,128)S(1)} %bitcast.29, s32[8,6]{1,0:T(8,128)S(1)} %copy-done.7, f32[8,6]{1,0:T(8,128)S(1)} %copy-done.8, ...), custom_call_target="tpu_custom_call" | custom-call | flops 1000000000 | bytes 10000000 | tf_op jit(solution)/shard_map/pallas_call | solution.py:318
  62.5 0.6 copy.43
  (38 shorter events, 0.2 us)
Async XLA Ops:
  0.6 29.1 %copy-start = (bf16[1024,1024]{1,0:T(8,128)(2,1)S(1)}, bf16[1024,1024]{1,0:T(8,128)(2,1)}, u32[]{:S(2)}) copy-start(bf16[1024,1024]{1,0:T(8,128)(2,1)} %param.35) | copy-start | bytes 6291460
  0.6 12.4 %copy-start.13 = (bf16[8,3,512]{2,0,1:T(8,128)(2,1)S(1)}, bf16[8,3,512]{2,0,1:T(8,128)(2,1)}, u32[]{:S(2)}) copy-start(bf16[8,3,512]{2,0,1:T(8,128)(2,1)} %param.33) | copy-start | bytes 73732
  0.7 12.4 %copy-start.12 = (bf16[8,3,512]{2,0,1:T(8,128)(2,1)S(1)}, bf16[8,3,512]{2,0,1:T(8,128)(2,1)}, u32[]{:S(2)}) copy-start(bf16[8,3,512]{2,0,1:T(8,128)(2,1)} %param.32) | copy-start | bytes 73732
  0.7 11.6 %copy-start.11 = (bf16[8,3,1024]{2,0,1:T(8,128)(2,1)S(1)}, bf16[8,3,1024]{2,0,1:T(8,128)(2,1)}, u32[]{:S(2)}) copy-start(bf16[8,3,1024]{2,0,1:T(8,128)(2,1)} %param.31) | copy-start | bytes 147460
  0.7 14.4 %copy-start.17 = (bf16[512,64]{0,1:T(8,128)(2,1)S(1)}, bf16[512,64]{0,1:T(8,128)(2,1)}, u32[]{:S(2)}) copy-start(bf16[512,64]{0,1:T(8,128)(2,1)} %param.56) | copy-start | bytes 196612
  0.7 14.0 %copy-start.16 = (bf16[64,512]{1,0:T(8,128)(2,1)S(1)}, bf16[64,512]{1,0:T(8,128)(2,1)}, u32[]{:S(2)}) copy-start(bf16[64,512]{1,0:T(8,128)(2,1)} %param.55) | copy-start | bytes 196612
  0.7 13.7 %copy-start.15 = (bf16[64,512]{1,0:T(8,128)(2,1)S(1)}, bf16[64,512]{1,0:T(8,128)(2,1)}, u32[]{:S(2)}) copy-start(bf16[64,512]{1,0:T(8,128)(2,1)} %param.54) | copy-start | bytes 196612
  0.7 11.6 %copy-start.18 = (bf16[4,1024]{1,0:T(4,128)(2,1)S(1)}, bf16[4,1024]{1,0:T(4,128)(2,1)}, u32[]{:S(2)}) copy-start(bf16[4,1024]{1,0:T(4,128)(2,1)} %param.42) | copy-start | bytes 24580
  15.6 5.9 %copy-start.10 = (f32[8,4,4,128]{3,2,1,0:T(4,128)S(1)}, f32[8,4,4,128]{3,2,1,0:T(4,128)}, u32[]{:S(2)}) copy-start(f32[8,4,4,128]{3,2,1,0:T(4,128)} %broadcast_in_dim.20) | copy-start | bytes 196612
  19.5 2.0 %copy-start.9 = (f32[8,16,64,128]{3,2,1,0:T(8,128)}, f32[8,16,64,128]{3,2,1,0:T(8,128)S(1)}, u32[]{:S(2)}) copy-start(f32[8,16,64,128]{3,2,1,0:T(8,128)S(1)} %multiply_add_fusion) | copy-start | bytes 12582916
  21.5 6.7 %copy-start.20 = (f32[16]{0:T(128)S(1)}, f32[16]{0:T(128)}, u32[]{:S(2)}) copy-start(f32[16]{0:T(128)} %param.41) | copy-start | bytes 196
  21.5 8.3 %copy-start.2 = (bf16[8,1024]{1,0:T(8,128)(2,1)S(1)}, bf16[8,1024]{1,0:T(8,128)(2,1)}, u32[]{:S(2)}) copy-start(bf16[8,1024]{1,0:T(8,128)(2,1)} %tokens_ref.1) | copy-start | bytes 49156
  21.5 8.3 %copy-start.14 = (f32[1024]{0:T(1024)S(1)}, f32[1024]{0:T(1024)}, u32[]{:S(2)}) copy-start(f32[1024]{0:T(1024)} %param.45) | copy-start | bytes 12292
  21.5 8.9 %copy-start.19 = (f32[1024]{0:T(1024)S(1)}, f32[1024]{0:T(1024)}, u32[]{:S(2)}) copy-start(f32[1024]{0:T(1024)} %param.46) | copy-start | bytes 12292
  21.5 8.9 %copy-start.3 = (bf16[1,1024,256]{2,1,0:T(8,128)(2,1)S(1)}, bf16[1,1024,256]{2,1,0:T(8,128)(2,1)}, u32[]{:S(2)}) copy-start(bf16[1,1024,256]{2,1,0:T(8,128)(2,1)} %gate_hbm.1) | copy-start | bytes 1572868
  21.5 8.9 %copy-start.4 = (bf16[1,1024,256]{2,1,0:T(8,128)(2,1)S(1)}, bf16[1,1024,256]{2,1,0:T(8,128)(2,1)}, u32[]{:S(2)}) copy-start(bf16[1,1024,256]{2,1,0:T(8,128)(2,1)} %up_hbm.1) | copy-start | bytes 1572868
  21.5 8.9 %copy-start.6 = (f32[1024]{0:T(1024)S(1)}, f32[1024]{0:T(1024)}, u32[]{:S(2)}) copy-start(f32[1024]{0:T(1024)} %param.48) | copy-start | bytes 12292
  21.5 8.9 %copy-start.7 = (s32[8,6]{1,0:T(8,128)S(1)}, s32[8,6]{1,0:T(8,128)}, u32[]{:S(2)}) copy-start(s32[8,6]{1,0:T(8,128)} %ids_ref.1) | copy-start | bytes 580
  21.6 8.9 %copy-start.8 = (f32[8,6]{1,0:T(8,128)S(1)}, f32[8,6]{1,0:T(8,128)}, u32[]{:S(2)}) copy-start(f32[8,6]{1,0:T(8,128)} %weights_ref.1) | copy-start | bytes 580
  30.5 1.6 %copy-start.1 = (bf16[1024,1024]{1,0:T(8,128)(2,1)S(1)}, bf16[1024,1024]{1,0:T(8,128)(2,1)}, u32[]{:S(2)}) copy-start(bf16[1024,1024]{1,0:T(8,128)(2,1)} %w_out_hbm.1) | copy-start | bytes 6291460
  32.1 1.0 %copy-start.5 = (bf16[1,256,1024]{2,1,0:T(8,128)(2,1)S(1)}, bf16[1,256,1024]{2,1,0:T(8,128)(2,1)}, u32[]{:S(2)}) copy-start(bf16[1,256,1024]{2,1,0:T(8,128)(2,1)} %down_hbm.1) | copy-start | bytes 1572868

commit v2 on v1

--- a/solution.py
+++ b/solution.py
@@ -14,22 +14,150 @@
     return values * lax.rsqrt(jnp.mean(values * values, axis=-1, keepdims=True) + epsilon) * gain
 
 
-def short_conv(previous, fresh, taps):
-    window = jnp.concatenate((previous, fresh[:, None]), axis=1)
-    summed = jnp.sum(window.astype(jnp.float32) * taps.astype(jnp.float32)[None], axis=1)
-    return (jax.nn.silu(summed), window[:, 1:])
-
-
-def mixer_core(
-    x_new,
-    z_new,
-    b_new,
-    c_new,
-    dt_raw,
+def mixer_kernel(
+    tokens_ref,
+    gain_ref,
+    state_hbm,
+    prev_x_ref,
+    prev_b_ref,
+    prev_c_ref,
+    wx_hbm,
+    wz_hbm,
+    wb_hbm,
+    wc_hbm,
+    wdt_ref,
+    bias_ref,
+    a_log_ref,
+    skip_ref,
+    taps_x_ref,
+    taps_b_ref,
+    taps_c_ref,
+    group_gain_ref,
+    mixed_ref,
+    state_out,
+    next_x_ref,
+    next_b_ref,
+    next_c_ref,
+    wx,
+    wz,
+    wb,
+    wc,
+    state,
+    w_sem,
+    in_sem,
+    out_sem,
+):
+    seqs, heads, head_dim, state_dim = state.shape
+    groups = wb.shape[1] // state_dim
+    per_group = heads // groups
+    inner = heads * head_dim
+    fetch = [
+        pltpu.make_async_copy(hbm, vmem, w_sem.at[i])
+        for i, (hbm, vmem) in enumerate(((wx_hbm, wx), (wb_hbm, wb), (wc_hbm, wc), (wz_hbm, wz)))
+    ]
+    fetch_state = [
+        pltpu.make_async_copy(state_hbm.at[s], state.at[s], in_sem.at[s]) for s in range(seqs)
+    ]
+    put_state = [
+        pltpu.make_async_copy(state.at[s], state_out.at[s], out_sem.at[s]) for s in range(seqs)
+    ]
+    for copy in fetch[:3] + fetch_state + fetch[3:]:
+        copy.start()
+
+    def project(weights):
+        out = jnp.dot(normed, weights, preferred_element_type=jnp.float32)
+        return out.astype(jnp.bfloat16).astype(jnp.float32)
+
+    def conv(prev_ref, fresh, taps_ref, next_ref):
+        prev = prev_ref[...].astype(jnp.float32)
+        taps = taps_ref[...].astype(jnp.float32)
+        depth = prev.shape[1]
+        summed = prev[:, 0, :] * taps[0:1]
+        for j in range(1, depth):
+            summed = summed + prev[:, j, :] * taps[j : j + 1]
+        summed = summed + fresh * taps[depth : depth + 1]
+        shifted = jnp.concatenate((prev[:, 1:, :], fresh[:, None, :]), axis=1)
+        next_ref[...] = shifted.astype(jnp.bfloat16)
+        return jax.nn.silu(summed)
+
+    normed = rms_rows(tokens_ref[...].astype(jnp.float32), gain_ref[...]).astype(jnp.bfloat16)
+    all_dt = jnp.dot(normed, wdt_ref[...], preferred_element_type=jnp.float32)
+    dt_raw = all_dt[:, :heads]
+    for t in range(1, all_dt.shape[1] // heads):
+        own = lax.axis_index("tp") == t
+        dt_raw = jnp.where(own, all_dt[:, t * heads : (t + 1) * heads], dt_raw)
+    step = jax.nn.softplus(dt_raw + bias_ref[...])
+    decay = jnp.exp(-step * jnp.exp(a_log_ref[...]))
+    spread = lax.broadcasted_iota(jnp.int32, (heads, inner), 1) // head_dim
+    spread = spread == lax.broadcasted_iota(jnp.int32, (heads, inner), 0)
+    per_head = jnp.concatenate((step, jnp.broadcast_to(skip_ref[...], step.shape)), axis=0)
+    wide = jnp.dot(
+        per_head,
+        spread.astype(jnp.float32),
+        precision=lax.Precision.HIGHEST,
+        preferred_element_type=jnp.float32,
+    )
+
+    fetch[0].wait()
+    xs = conv(prev_x_ref, project(wx[...]), taps_x_ref, next_x_ref)
+    fetch[1].wait()
+    bs = conv(prev_b_ref, project(wb[...]), taps_b_ref, next_b_ref)
+    fetch[2].wait()
+    cs = conv(prev_c_ref, project(wc[...]), taps_c_ref, next_c_ref)
+    stepped = jnp.transpose(wide[:seqs] * xs)
+    cs_high = cs.astype(jnp.bfloat16)
+    cs_low = (cs - cs_high.astype(jnp.float32)).astype(jnp.bfloat16)
+    cs_pair = jnp.concatenate((cs_high, cs_low), axis=0)
+
+    row = lax.broadcasted_iota(jnp.int32, (seqs, per_group * head_dim), 0)
+    read = [jnp.zeros(row.shape, jnp.float32) for _ in range(groups)]
+    for s in range(seqs):
+        fetch_state[s].wait()
+        for g in range(groups):
+            span = slice(g * state_dim, (g + 1) * state_dim)
+            fresh = []
+            for h in range(g * per_group, (g + 1) * per_group):
+                new = (
+                    decay[s : s + 1, h : h + 1] * state[s, h]
+                    + stepped[h * head_dim : (h + 1) * head_dim, s : s + 1] * bs[s : s + 1, span]
+                )
+                state[s, h] = new
+                fresh.append(new.astype(jnp.bfloat16))
+            both = lax.dot_general(
+                cs_pair[:, span],
+                jnp.concatenate(fresh, axis=0),
+                (((1,), (1,)), ((), ())),
+                preferred_element_type=jnp.float32,
+            )
+            read[g] = jnp.where(row == s, both[:seqs] + both[seqs:], read[g])
+        if s > 0:
+            put_state[s - 1].start()
+    fetch[3].wait()
+    gate = jax.nn.silu(project(wz[...]))
+    put_state[seqs - 1].start()
+    gated = (jnp.concatenate(read, axis=1) + wide[seqs:] * xs) * gate
+    block = inner // groups
+    for g in range(groups):
+        span = slice(g * block, (g + 1) * block)
+        part = gated[:, span]
+        part = part * lax.rsqrt(jnp.mean(part * part, axis=-1, keepdims=True) + epsilon)
+        mixed_ref[:, span] = (part * group_gain_ref[:, span]).astype(jnp.bfloat16)
+    for copy in put_state:
+        copy.wait()
+
+
+def mixer(
+    tokens,
+    norm1_gain,
     ssm_state,
     conv_x,
     conv_b,
     conv_c,
+    w_x,
+    w_z,
+    w_b,
+    w_c,
+    w_dt,
     dt_bias,
     a_log,
     d_skip,
@@ -38,29 +166,53 @@
     taps_c,
     group_gain,
 ):
-    seqs, heads, head_dim, state_dim = ssm_state.shape
-    groups = b_new.shape[1] // state_dim
-    x_conv, conv_x_next = short_conv(conv_x, x_new, taps_x)
-    b_conv, conv_b_next = short_conv(conv_b, b_new, taps_b)
-    c_conv, conv_c_next = short_conv(conv_c, c_new, taps_c)
-    x_heads = x_conv.reshape(seqs, heads, head_dim)
-    b_heads = jnp.repeat(b_conv.reshape(seqs, groups, state_dim), heads // groups, axis=1)
-    c_heads = jnp.repeat(c_conv.reshape(seqs, groups, state_dim), heads // groups, axis=1)
-    step = jax.nn.softplus(dt_raw + dt_bias)
-    decay = jnp.exp(-step * jnp.exp(a_log))
-    state_next = (
-        decay[:, :, None, None] * ssm_state
-        + (step[:, :, None] * x_heads)[:, :, :, None] * b_heads[:, :, None, :]
-    )
-    readout = (
-        jnp.einsum("shpn,shn->shp", state_next, c_heads, precision=lax.Precision.HIGHEST)
-        + d_skip[None, :, None] * x_heads
-    )
-    gated = readout.reshape(seqs, heads * head_dim) * jax.nn.silu(z_new.astype(jnp.float32))
-    grouped = gated.reshape(seqs, groups, -1)
-    grouped = grouped * lax.rsqrt(jnp.mean(grouped * grouped, axis=-1, keepdims=True) + epsilon)
-    mixed_heads = (grouped.reshape(seqs, heads * head_dim) * group_gain).astype(jnp.bfloat16)
-    return (mixed_heads, state_next, conv_x_next, conv_b_next, conv_c_next)
+    seqs = tokens.shape[0]
+    vmem = pl.BlockSpec(memory_space=pltpu.VMEM)
+    hbm = pl.BlockSpec(memory_space=pl.ANY)
+    shape = jax.ShapeDtypeStruct
+    return pl.pallas_call(
+        mixer_kernel,
+        out_shape=(
+            shape((seqs, w_x.shape[1]), jnp.bfloat16),
+            shape(ssm_state.shape, ssm_state.dtype),
+            shape(conv_x.shape, conv_x.dtype),
+            shape(conv_b.shape, conv_b.dtype),
+            shape(conv_c.shape, conv_c.dtype),
+        ),
+        in_specs=[vmem, vmem, hbm, vmem, vmem, vmem, hbm, hbm, hbm, hbm] + [vmem] * 8,
+        out_specs=(vmem, hbm, vmem, vmem, vmem),
+        scratch_shapes=[
+            pltpu.VMEM(w_x.shape, jnp.bfloat16),
+            pltpu.VMEM(w_z.shape, jnp.bfloat16),
+            pltpu.VMEM(w_b.shape, jnp.bfloat16),
+            pltpu.VMEM(w_c.shape, jnp.bfloat16),
+            pltpu.VMEM(ssm_state.shape, jnp.float32),
+            pltpu.SemaphoreType.DMA((4,)),
+            pltpu.SemaphoreType.DMA((seqs,)),
+            pltpu.SemaphoreType.DMA((seqs,)),
+        ],
+        compiler_params=pltpu.CompilerParams(vmem_limit_bytes=48 * 1024 * 1024),
+        cost_estimate=pl.CostEstimate(flops=10**8, bytes_accessed=14 * 10**6, transcendentals=0),
+    )(
+        tokens,
+        norm1_gain[None],
+        ssm_state,
+        conv_x,
+        conv_b,
+        conv_c,
+        w_x,
+        w_z,
+        w_b,
+        w_c,
+        w_dt,
+        dt_bias[None],
+        a_log[None],
+        d_skip[None],
+        taps_x,
+        taps_b,
+        taps_c,
+        group_gain[None],
+    )
 
 
 def tail_kernel(
@@ -392,25 +544,18 @@
     dense_down,
     branch_gate,
 ):
-    stream = tokens.astype(jnp.float32)
-    normed = rms_rows(stream, norm1_gain).astype(jnp.bfloat16)
-    x_proj = jnp.dot(normed, w_x, preferred_element_type=jnp.float32).astype(jnp.bfloat16)
-    z_proj = jnp.dot(normed, w_z, preferred_element_type=jnp.float32).astype(jnp.bfloat16)
-    b_proj = jnp.dot(normed, w_b, preferred_element_type=jnp.float32).astype(jnp.bfloat16)
-    c_proj = jnp.dot(normed, w_c, preferred_element_type=jnp.float32).astype(jnp.bfloat16)
-    local_heads = ssm_state.shape[1]
-    dt_columns = lax.dynamic_slice_in_dim(w_dt, lax.axis_index("tp") * local_heads, local_heads, 1)
-    dt_raw = jnp.dot(normed, dt_columns, preferred_element_type=jnp.float32)
-    mixed_heads, state_next, conv_x_next, conv_b_next, conv_c_next = mixer_core(
-        x_proj,
-        z_proj,
-        b_proj,
-        c_proj,
-        dt_raw,
+    mixed_heads, state_next, conv_x_next, conv_b_next, conv_c_next = mixer(
+        tokens,
+        norm1_gain,
         ssm_state,
         conv_x,
         conv_b,
         conv_c,
+        w_x,
+        w_z,
+        w_b,
+        w_c,
+        w_dt,
         dt_bias,
         a_log,
         d_skip,

time: 63.8 us -> 63 us (0.987)
  local copies, waits for them, and re-layouts: 9.54 us -> 24 us
  matrix products: 13.1 us -> 0 us
  other arithmetic: 10 us -> 1.98 us
  Pallas kernels: 29.3 us -> 35.3 us
    dot_general x6 -> x0, matrix products: 13.1 us -> none  [the longest x1 6.58 us: mixer_core(): jnp.einsum('shpn,shn->shp', state_next, c_heads, precision=lax.Precision....]
    unnamed x46 -> x53, local copies, waits for them, and re-layouts: 5.69 us -> 17.3 us
    pallas_call x0 -> x1, Pallas kernels: none -> 5.94 us  [mixer(): pl.pallas_call(mixer_kernel, out_shape=(shape((seqs, w_x.shape[1]), jnp.b...]
    add x2 -> x0, other arithmetic: 4.53 us -> none  [the longest x1 3.82 us: mixer_core(): decay[:, :, None, None] * ssm_state]
    reduce_sum x5 -> x0, other arithmetic: 2.45 us -> none  [the longest x3 1.52 us: short_conv(): jnp.sum(window.astype(jnp.float32) * taps.astype(jnp.float32)[None], axis=1)]
    reshape x2, local copies, waits for them, and re-layouts: 0.36 us -> 2.81 us  [after_mixer(): by_owner = lambda w: w.reshape(depth, peers, share).transpose(1, 0, 2)]
    concatenate x1, other arithmetic: 0.26 us -> 1.98 us  [after_mixer(): jnp.concatenate((by_owner(dense_gate), by_owner(dense_up), dense_down.res...]
    reshape x1, local copies, waits for them, and re-layouts: 0.18 us -> 1.74 us  [after_mixer(): dense_down.reshape(peers, share, depth).transpose(0, 2, 1)]
where the time goes in v2:
time: 63 us; the launch traced here: 62.2 us
  Pallas kernels  35.3 us (56%)
  local copies, waits for them, and re-layouts  24 us (38%)
  other arithmetic  1.98 us (3%)
  between operations  0.86 us (1%)
    pallas_call x1, Pallas kernels, after_mixer(): pl.pallas_call(functools.partial(tail_kernel, peers, splits, share), out_...  29.4 us
    unnamed x53, local copies, waits for them, and re-layouts  17.3 us
    pallas_call x1, Pallas kernels, mixer(): pl.pallas_call(mixer_kernel, out_shape=(shape((seqs, w_x.shape[1]), jnp.b...  5.94 us
    reshape x2, local copies, waits for them, and re-layouts, after_mixer(): by_owner = lambda w: w.reshape(depth, peers, share).transpose(1, 0, 2)  2.81 us
    concatenate x1, other arithmetic, after_mixer(): jnp.concatenate((by_owner(dense_gate), by_owner(dense_up), dense_down.res...  1.98 us
    reshape x1, local copies, waits for them, and re-layouts, after_mixer(): dense_down.reshape(peers, share, depth).transpose(0, 2, 1)  1.74 us
    broadcast_in_dim x1, local copies, waits for them, and re-layouts, after_mixer(): branch_gate[None]  1.59 us

profile of v2, /device:TPU:0, one launch (start us, length us, event | category | flops | bytes accessed | tf_op | source)
XLA Modules:
  0.0 62.2 jit_solution(9858848353562610291)
XLA Ops:
  0.6 0.0 copy-start.8
  0.6 0.0 copy-start.2
  0.7 0.0 copy-start
  0.7 0.6 pad.3.clone
  1.3 1.6 %broadcast_in_dim.31.branch_ref = bf16[1,1024]{1,0:T(2,128)(2,1)} reshape(bf16[1024]{0:T(1024)(128)(2,1)} %param.57) | data formatting | bytes 4096 | tf_op jit(solution)/shard_map/broadcast_in_dim | solution.py:512
  2.8 0.8 %copy.42.prev_b_ref = bf16[8,3,512]{2,1,0:T(4,128)(2,1)S(1)} copy(bf16[8,3,512]{2,0,1:T(8,128)(2,1)} %param.32) | data formatting | bytes 49152 | tf_op args[3]
  3.6 0.8 %copy.43.prev_c_ref = bf16[8,3,512]{2,1,0:T(4,128)(2,1)S(1)} copy(bf16[8,3,512]{2,0,1:T(8,128)(2,1)} %param.33) | data formatting | bytes 49152 | tf_op args[4]
  4.4 0.8 %copy.41.prev_x_ref = bf16[8,3,1024]{2,1,0:T(4,128)(2,1)S(1)} copy(bf16[8,3,1024]{2,0,1:T(8,128)(2,1)} %param.31) | data formatting | bytes 98304 | tf_op args[2]
  5.2 1.6 %copy.45 = bf16[64,512]{0,1:T(8,128)(2,1)} copy(bf16[64,512]{1,0:T(8,128)(2,1)} %param.54) | data formatting | bytes 131072 | tf_op args[25]
  6.8 1.1 %copy.46 = bf16[64,16,32]{2,0,1:T(8,128)(2,1)S(1)} copy(bf16[64,16,32]{0,2,1:T(8,128)(2,1)} %bitcast.21) | data formatting | bytes 131072 | tf_op jit(solution)/shard_map/reshape | solution.py:457
  7.9 1.6 %copy.47 = bf16[64,512]{0,1:T(8,128)(2,1)} copy(bf16[64,512]{1,0:T(8,128)(2,1)} %param.55) | data formatting | bytes 131072 | tf_op args[26]
  9.5 1.7 %copy.48 = bf16[64,16,32]{2,0,1:T(8,128)(2,1)} copy(bf16[64,16,32]{0,2,1:T(8,128)(2,1)} %bitcast.22) | data formatting | bytes 131072 | tf_op jit(solution)/shard_map/reshape | solution.py:457
  11.2 1.6 %copy.49 = bf16[512,64]{1,0:T(8,128)(2,1)} copy(bf16[512,64]{0,1:T(8,128)(2,1)} %param.56) | data formatting | bytes 131072 | tf_op args[27]
  12.8 1.7 %copy.50 = bf16[16,32,64]{1,2,0:T(8,128)(2,1)} copy(bf16[16,32,64]{2,1,0:T(8,128)(2,1)} %bitcast.23) | data formatting | bytes 131072 | tf_op jit(solution)/shard_map/reshape | solution.py:462
  14.6 2.0 %maximum_maximum_fusion.stage_ref = bf16[16,64,128]{2,1,0:T(8,128)(2,1)} fusion(bf16[16,64,32]{2,1,0:T(8,128)(2,1)} %bitcast.20, bf16[16,64,32]{2,1,0:T(8,128)(2,1)} %bitcast.19, bf16[16,64,32]{2,1,0:T(8,128)(2,1)S(1)} %bitcast.18, bf16[128]{0:T(256)(128)(2,1)} %pad.3.clone), kind=kLoop, calls=%fused_computation | loop fusion | flops 1048576 | bytes 459008 | tf_op jit(solution)/shard_map/concatenate | solution.py:458
  16.5 1.0 %copy.44.wdt_ref = bf16[1024,32]{1,0:T(8,128)(2,1)S(1)} copy(bf16[1024,32]{0,1:T(8,128)(2,1)} %param.38) | data formatting | bytes 131072 | tf_op args[9]
  17.6 0.0 copy-done.8
  17.6 0.0 copy-done.2
  17.6 0.0 copy-done
  17.6 0.0 copy-start.3
  17.6 1.2 %copy-done.3 = bf16[1024,512]{1,0:T(8,128)(2,1)S(1)} copy-done((bf16[1024,512]{1,0:T(8,128)(2,1)S(1)}, bf16[1024,512]{1,0:T(8,128)(2,1)}, u32[]{:S(2)}) %copy-start.3) | copy-done | bytes 1048600
  18.8 0.7 %copy-done.10 = bf16[4,1024]{1,0:T(4,128)(2,1)S(1)} copy-done((bf16[4,1024]{1,0:T(4,128)(2,1)S(1)}, bf16[4,1024]{1,0:T(4,128)(2,1)}, u32[]{:S(2)}) %copy-start.10) | copy-done | bytes 8216
  19.5 0.7 %copy-done.11 = f32[1024]{0:T(1024)S(1)} copy-done((f32[1024]{0:T(1024)S(1)}, f32[1024]{0:T(1024)}, u32[]{:S(2)}) %copy-start.11) | copy-done | bytes 4120
  20.2 0.7 %copy-done.12 = bf16[4,512]{1,0:T(4,128)(2,1)S(1)} copy-done((bf16[4,512]{1,0:T(4,128)(2,1)S(1)}, bf16[4,512]{1,0:T(4,128)(2,1)}, u32[]{:S(2)}) %copy-start.12) | copy-done | bytes 4120
  20.9 0.7 %copy-done.13 = bf16[4,512]{1,0:T(4,128)(2,1)S(1)} copy-done((bf16[4,512]{1,0:T(4,128)(2,1)S(1)}, bf16[4,512]{1,0:T(4,128)(2,1)}, u32[]{:S(2)}) %copy-start.13) | copy-done | bytes 4120
  21.6 0.7 %copy-done.14 = f32[1024]{0:T(1024)S(1)} copy-done((f32[1024]{0:T(1024)S(1)}, f32[1024]{0:T(1024)}, u32[]{:S(2)}) %copy-start.14) | copy-done | bytes 4120
  22.3 0.7 %copy-done.18 = f32[16]{0:T(128)S(1)} copy-done((f32[16]{0:T(128)S(1)}, f32[16]{0:T(128)}, u32[]{:S(2)}) %copy-start.18) | copy-done | bytes 88
  22.9 0.7 %copy-done.19 = f32[16]{0:T(128)S(1)} copy-done((f32[16]{0:T(128)S(1)}, f32[16]{0:T(128)}, u32[]{:S(2)}) %copy-start.19) | copy-done | bytes 88
  23.6 0.7 %copy-done.20 = f32[16]{0:T(128)S(1)} copy-done((f32[16]{0:T(128)S(1)}, f32[16]{0:T(128)}, u32[]{:S(2)}) %copy-start.20) | copy-done | bytes 88
  24.2 0.0 copy-start.7
  24.2 0.0 copy-start.9
  24.3 0.0 copy-start.15
  24.3 0.0 copy-start.16
  24.3 0.0 copy-start.17
  24.3 5.9 %shard_map.308 = (bf16[8,1024]{1,0:T(8,128)(2,1)S(1)}, f32[8,16,64,128]{3,2,1,0:T(8,128)}, bf16[8,3,1024]{2,1,0:T(4,128)(2,1)S(1)}, bf16[8,3,512]{2,1,0:T(4,128)(2,1)S(1)}, bf16[8,3,512]{2,1,0:T(4,128)(2,1)S(1)}) custom-call(bf16[8,1024]{1,0:T(8,128)(2,1)S(1)} %copy-done.8, f32[1,1024]{1,0:T(1,128)S(1)} %bitcast.12, f32[8,16,64,128]{3,2,1,0:T(8,128)} %state_hbm.1, ...), custom_call_target="tpu_custom_call" | custom-call | flops 100000000 | bytes 14000000 | tf_op jit(solution)/shard_map/pallas_call | solution.py:173
  30.2 0.0 copy-done.1
  30.3 0.0 copy-done.4
  30.3 0.0 copy-done.5
  30.3 0.0 copy-done.6
  30.3 0.0 copy-done.7
  30.3 0.0 copy-done.9
  30.3 0.0 copy-done.15
  30.3 0.0 copy-done.16
  30.3 29.4 %shard_map.309 = bf16[8,512]{1,0:T(8,128)(2,1)S(1)} custom-call(bf16[8,1024]{1,0:T(8,128)(2,1)S(1)} %get-tuple-element.10.mixed_ref, bf16[1024,1024]{1,0:T(8,128)(2,1)S(1)} %copy-done.1, bf16[8,1024]{1,0:T(8,128)(2,1)S(1)} %copy-done.8, f32[1,1024]{1,0:T(1,128)S(1)} %bitcast.14, s32[8,6]{1,0:T(8,128)S(1)} %copy-done.16, f32[8,6]{1,0:T(8,128)S(1)} %copy-done.17, ...), custom_call_target="tpu_custom_call" | custom-call | flops 1000000000 | bytes 10000000 | tf_op jit(solution)/shard_map/pallas_call | solution.py:470
  59.7 0.6 copy.52
  60.3 0.6 copy.53
  60.9 0.6 %copy.51 = bf16[8,3,1024]{2,0,1:T(8,128)(2,1)} copy(bf16[8,3,1024]{2,1,0:T(4,128)(2,1)S(1)} %get-tuple-element.22) | data formatting | bytes 98304
  61.6 0.6 copy.55
  (14 shorter events, 0.0 us)
Async XLA Ops:
  0.6 16.9 %copy-start.8 = (bf16[8,1024]{1,0:T(8,128)(2,1)S(1)}, bf16[8,1024]{1,0:T(8,128)(2,1)}, u32[]{:S(2)}) copy-start(bf16[8,1024]{1,0:T(8,128)(2,1)} %tokens_ref.3) | copy-start | bytes 49156
  0.6 16.9 %copy-start.2 = (bf16[1024,512]{1,0:T(8,128)(2,1)S(1)}, bf16[1024,512]{1,0:T(8,128)(2,1)}, u32[]{:S(2)}) copy-start(bf16[1024,512]{1,0:T(8,128)(2,1)} %wb_hbm.1) | copy-start | bytes 3145732
  0.7 16.9 %copy-start = (bf16[1024,1024]{1,0:T(8,128)(2,1)S(1)}, bf16[1024,1024]{1,0:T(8,128)(2,1)}, u32[]{:S(2)}) copy-start(bf16[1024,1024]{1,0:T(8,128)(2,1)} %wx_hbm.1) | copy-start | bytes 6291460
  17.6 1.2 %copy-start.3 = (bf16[1024,512]{1,0:T(8,128)(2,1)S(1)}, bf16[1024,512]{1,0:T(8,128)(2,1)}, u32[]{:S(2)}) copy-start(bf16[1024,512]{1,0:T(8,128)(2,1)} %wc_hbm.1) | copy-start | bytes 3145732
  18.8 0.7 %copy-start.10 = (bf16[4,1024]{1,0:T(4,128)(2,1)S(1)}, bf16[4,1024]{1,0:T(4,128)(2,1)}, u32[]{:S(2)}) copy-start(bf16[4,1024]{1,0:T(4,128)(2,1)} %taps_x_ref.1) | copy-start | bytes 24580
  19.5 0.7 %copy-start.11 = (f32[1024]{0:T(1024)S(1)}, f32[1024]{0:T(1024)}, u32[]{:S(2)}) copy-start(f32[1024]{0:T(1024)} %param.45) | copy-start | bytes 12292
  20.2 0.7 %copy-start.12 = (bf16[4,512]{1,0:T(4,128)(2,1)S(1)}, bf16[4,512]{1,0:T(4,128)(2,1)}, u32[]{:S(2)}) copy-start(bf16[4,512]{1,0:T(4,128)(2,1)} %taps_b_ref.1) | copy-start | bytes 12292
  20.9 0.7 %copy-start.13 = (bf16[4,512]{1,0:T(4,128)(2,1)S(1)}, bf16[4,512]{1,0:T(4,128)(2,1)}, u32[]{:S(2)}) copy-start(bf16[4,512]{1,0:T(4,128)(2,1)} %taps_c_ref.1) | copy-start | bytes 12292
  21.6 0.7 %copy-start.14 = (f32[1024]{0:T(1024)S(1)}, f32[1024]{0:T(1024)}, u32[]{:S(2)}) copy-start(f32[1024]{0:T(1024)} %param.46) | copy-start | bytes 12292
  22.3 0.7 %copy-start.18 = (f32[16]{0:T(128)S(1)}, f32[16]{0:T(128)}, u32[]{:S(2)}) copy-start(f32[16]{0:T(128)} %param.39) | copy-start | bytes 196
  22.9 0.7 %copy-start.19 = (f32[16]{0:T(128)S(1)}, f32[16]{0:T(128)}, u32[]{:S(2)}) copy-start(f32[16]{0:T(128)} %param.40) | copy-start | bytes 196
  23.6 0.7 %copy-start.20 = (f32[16]{0:T(128)S(1)}, f32[16]{0:T(128)}, u32[]{:S(2)}) copy-start(f32[16]{0:T(128)} %param.41) | copy-start | bytes 196
  24.2 6.0 %copy-start.1 = (bf16[1024,1024]{1,0:T(8,128)(2,1)S(1)}, bf16[1024,1024]{1,0:T(8,128)(2,1)}, u32[]{:S(2)}) copy-start(bf16[1024,1024]{1,0:T(8,128)(2,1)} %w_out_hbm.1) | copy-start | bytes 6291460
  24.2 6.0 %copy-start.4 = (bf16[16,64,128]{2,1,0:T(8,128)(2,1)S(1)}, bf16[16,64,128]{2,1,0:T(8,128)(2,1)}, u32[]{:S(2)}) copy-start(bf16[16,64,128]{2,1,0:T(8,128)(2,1)} %maximum_maximum_fusion.stage_ref) | copy-start | bytes 786436
  24.2 6.0 %copy-start.5 = (bf16[1,1024,256]{2,1,0:T(8,128)(2,1)S(1)}, bf16[1,1024,256]{2,1,0:T(8,128)(2,1)}, u32[]{:S(2)}) copy-start(bf16[1,1024,256]{2,1,0:T(8,128)(2,1)} %gate_hbm.1) | copy-start | bytes 1572868
  24.2 6.0 %copy-start.6 = (bf16[1,1024,256]{2,1,0:T(8,128)(2,1)S(1)}, bf16[1,1024,256]{2,1,0:T(8,128)(2,1)}, u32[]{:S(2)}) copy-start(bf16[1,1024,256]{2,1,0:T(8,128)(2,1)} %up_hbm.1) | copy-start | bytes 1572868
  24.2 6.0 %copy-start.7 = (bf16[1,256,1024]{2,1,0:T(8,128)(2,1)S(1)}, bf16[1,256,1024]{2,1,0:T(8,128)(2,1)}, u32[]{:S(2)}) copy-start(bf16[1,256,1024]{2,1,0:T(8,128)(2,1)} %down_hbm.1) | copy-start | bytes 1572868
  24.2 6.0 %copy-start.9 = (bf16[1,1024]{1,0:T(2,128)(2,1)S(1)}, bf16[1,1024]{1,0:T(2,128)(2,1)}, u32[]{:S(2)}) copy-start(bf16[1,1024]{1,0:T(2,128)(2,1)} %broadcast_in_dim.31.branch_ref) | copy-start | bytes 6148
  24.3 6.0 %copy-start.15 = (f32[1024]{0:T(1024)S(1)}, f32[1024]{0:T(1024)}, u32[]{:S(2)}) copy-start(f32[1024]{0:T(1024)} %param.48) | copy-start | bytes 12292
  24.3 6.0 %copy-start.16 = (s32[8,6]{1,0:T(8,128)S(1)}, s32[8,6]{1,0:T(8,128)}, u32[]{:S(2)}) copy-start(s32[8,6]{1,0:T(8,128)} %ids_ref.1) | copy-start | bytes 580
  24.3 6.0 %copy-start.17 = (f32[8,6]{1,0:T(8,128)S(1)}, f32[8,6]{1,0:T(8,128)}, u32[]{:S(2)}) copy-start(f32[8,6]{1,0:T(8,128)} %weights_ref.1) | copy-start | bytes 580

commit v3 on v2

--- a/solution.py
+++ b/solution.py
@@ -71,17 +71,19 @@
     def conv(prev_ref, fresh, taps_ref, next_ref):
         prev = prev_ref[...].astype(jnp.float32)
         taps = taps_ref[...].astype(jnp.float32)
-        depth = prev.shape[1]
-        summed = prev[:, 0, :] * taps[0:1]
+        depth = prev.shape[0]
+        summed = prev[0] * taps[0:1]
         for j in range(1, depth):
-            summed = summed + prev[:, j, :] * taps[j : j + 1]
+            summed = summed + prev[j] * taps[j : j + 1]
+            next_ref[j - 1] = prev[j].astype(jnp.bfloat16)
         summed = summed + fresh * taps[depth : depth + 1]
-        shifted = jnp.concatenate((prev[:, 1:, :], fresh[:, None, :]), axis=1)
-        next_ref[...] = shifted.astype(jnp.bfloat16)
+        next_ref[depth - 1] = fresh.astype(jnp.bfloat16)
         return jax.nn.silu(summed)
 
     normed = rms_rows(tokens_ref[...].astype(jnp.float32), gain_ref[...]).astype(jnp.bfloat16)
-    all_dt = jnp.dot(normed, wdt_ref[...], preferred_element_type=jnp.float32)
+    all_dt = lax.dot_general(
+        normed, wdt_ref[...], (((1,), (1,)), ((), ())), preferred_element_type=jnp.float32
+    )
     dt_raw = all_dt[:, :heads]
     for t in range(1, all_dt.shape[1] // heads):
         own = lax.axis_index("tp") == t
@@ -170,7 +172,9 @@
     vmem = pl.BlockSpec(memory_space=pltpu.VMEM)
     hbm = pl.BlockSpec(memory_space=pl.ANY)
     shape = jax.ShapeDtypeStruct
-    return pl.pallas_call(
+    taps_first = lambda a: a.transpose(1, 0, 2)
+    conv_x, conv_b, conv_c = taps_first(conv_x), taps_first(conv_b), taps_first(conv_c)
+    mixed, state, next_x, next_b, next_c = pl.pallas_call(
         mixer_kernel,
         out_shape=(
             shape((seqs, w_x.shape[1]), jnp.bfloat16),
@@ -191,7 +195,6 @@
             pltpu.SemaphoreType.DMA((seqs,)),
             pltpu.SemaphoreType.DMA((seqs,)),
         ],
-        compiler_params=pltpu.CompilerParams(vmem_limit_bytes=48 * 1024 * 1024),
         cost_estimate=pl.CostEstimate(flops=10**8, bytes_accessed=14 * 10**6, transcendentals=0),
     )(
         tokens,
@@ -204,7 +207,7 @@
         w_z,
         w_b,
         w_c,
-        w_dt,
+        w_dt.T,
         dt_bias[None],
         a_log[None],
         d_skip[None],
@@ -213,6 +216,7 @@
         taps_c,
         group_gain[None],
     )
+    return mixed, state, taps_first(next_x), taps_first(next_b), taps_first(next_c)
 
 
 def tail_kernel(
@@ -228,7 +232,9 @@
     gate_hbm,
     up_hbm,
     down_hbm,
-    stage_ref,
+    dense_gate_ref,
+    dense_up_ref,
+    dense_down_ref,
     branch_ref,
     out_ref,
     w_out,
@@ -237,6 +243,7 @@
     partials,
     features,
     tables,
+    stage_ref,
     dense,
     packed,
     returned,
@@ -288,6 +295,18 @@
     for k in range(ids_ref.shape[1]):
         table = table + jnp.where(lanes == ids_ref[:, k : k + 1], weights_ref[:, k : k + 1], 0.0)
     tables[ep] = table
+    lane = lax.broadcasted_iota(jnp.int32, stage_ref.shape[1:], 1)
+    for owner in range(peers):
+        start = owner * share
+        base = start // 128 * 128
+        block = jnp.zeros(stage_ref.shape[1:], jnp.float32)
+        for i, ref in enumerate((dense_gate_ref, dense_up_ref, dense_down_ref)):
+            source = ref[:, base : base + 128].astype(jnp.float32)
+            shift = (i * share - (start - base)) % 128
+            if shift:
+                source = pltpu.roll(source, shift, 1)
+            block = jnp.where((lane >= i * share) & (lane < (i + 1) * share), source, block)
+        stage_ref[owner] = block.astype(jnp.bfloat16)
     dense[ep] = stage_ref[ep]
 
     loads[0].wait()
@@ -454,23 +473,13 @@
     hidden = exp_gate.shape[2]
     part = width // splits
     lanes = -(-3 * share // 128) * 128
-    by_owner = lambda w: w.reshape(depth, peers, share).transpose(1, 0, 2)
-    stage = jnp.concatenate(
-        (
-            by_owner(dense_gate),
-            by_owner(dense_up),
-            dense_down.reshape(peers, share, depth).transpose(0, 2, 1),
-            jnp.zeros((peers, depth, lanes - 3 * share), jnp.bfloat16),
-        ),
-        axis=2,
-    )
     vmem = pl.BlockSpec(memory_space=pltpu.VMEM)
     hbm = pl.BlockSpec(memory_space=pl.ANY)
     dma = lambda count: pltpu.SemaphoreType.DMA((count,))
     return pl.pallas_call(
         functools.partial(tail_kernel, peers, splits, share),
         out_shape=jax.ShapeDtypeStruct((seqs, part), jnp.bfloat16),
-        in_specs=[vmem, hbm, vmem, vmem, vmem, vmem, hbm, hbm, hbm, vmem, vmem],
+        in_specs=[vmem, hbm, vmem, vmem, vmem, vmem, hbm, hbm, hbm, vmem, vmem, vmem, vmem],
         out_specs=vmem,
         scratch_shapes=[
             pltpu.VMEM(w_out.shape, jnp.bfloat16),
@@ -479,6 +488,7 @@
             pltpu.VMEM((splits, seqs, width), jnp.bfloat16),
             pltpu.VMEM((peers, seqs, width), jnp.bfloat16),
             pltpu.VMEM((peers, seqs, 128), jnp.float32),
+            pltpu.VMEM((peers, depth, lanes), jnp.bfloat16),
             pltpu.VMEM((peers, depth, lanes), jnp.bfloat16),
             pltpu.VMEM((splits, peers, seqs, part), jnp.bfloat16),
             pltpu.VMEM((peers * splits, seqs, part), jnp.bfloat16),
@@ -495,7 +505,7 @@
             dma(peers * splits),
         ],
         compiler_params=pltpu.CompilerParams(
-            collective_id=0, has_side_effects=True, vmem_limit_bytes=32 * 1024 * 1024
+            collective_id=0, has_side_effects=True
         ),
         cost_estimate=pl.CostEstimate(flops=10**9, bytes_accessed=10**7, transcendentals=0),
     )(
@@ -508,8 +518,10 @@
         exp_gate,
         exp_up,
         exp_down,
-        stage,
-        branch_gate[None],
+        dense_gate,
+        dense_up,
+        dense_down.T,
+        branch_gate.astype(jnp.float32)[None],
     )
 
 

time: 63 us -> 42.9 us (0.68)
  local copies, waits for them, and re-layouts: 24 us -> 1.3 us
  Pallas kernels: 35.3 us -> 39.4 us
  other arithmetic: 1.98 us -> 1.28 us
    unnamed x53 -> x1, local copies, waits for them, and re-layouts: 17.3 us -> 1.3 us
    reshape x3 -> x0, local copies, waits for them, and re-layouts: 4.55 us -> none  [the longest x2 2.81 us: after_mixer(): by_owner = lambda w: w.reshape(depth, peers, share).transpose(1, 0, 2)]
    pallas_call x1, Pallas kernels: 5.94 us -> 8.92 us  [mixer(): pl.pallas_call(mixer_kernel, out_shape=(shape((seqs, w_x.shape[1]), jnp.b...]
    concatenate x1 -> x0, other arithmetic: 1.98 us -> none  [after_mixer(): jnp.concatenate((by_owner(dense_gate), by_owner(dense_up), dense_down.res...]
    broadcast_in_dim x2 -> x0, local copies, waits for them, and re-layouts: 1.59 us -> none  [the longest x1 1.59 us: after_mixer(): branch_gate[None]]
    broadcast_in_dim x0 -> x1, other arithmetic: none -> 1.28 us  [after_mixer(): branch_gate.astype(jnp.float32)[None]]
    pallas_call x1, Pallas kernels: 29.4 us -> 30.5 us  [after_mixer(): pl.pallas_call(functools.partial(tail_kernel, peers, splits, share), out_...]
where the time goes in v3:
time: 42.9 us; the launch traced here: 42.6 us
  Pallas kernels  39.4 us (92%)
  local copies, waits for them, and re-layouts  1.3 us (3%)
  other arithmetic  1.28 us (3%)
  between operations  0.65 us (2%)
    pallas_call x1, Pallas kernels, after_mixer(): pl.pallas_call(functools.partial(tail_kernel, peers, splits, share), out_...  30.5 us
    pallas_call x1, Pallas kernels, mixer(): pl.pallas_call(mixer_kernel, out_shape=(shape((seqs, w_x.shape[1]), jnp.b...  8.92 us
    unnamed x1, local copies, waits for them, and re-layouts  1.3 us
    broadcast_in_dim x1, other arithmetic, after_mixer(): branch_gate.astype(jnp.float32)[None]  1.28 us

profile of v3, /device:TPU:0, one launch (start us, length us, event | category | flops | bytes accessed | tf_op | source)
XLA Modules:
  0.0 42.6 jit_solution(10092001844943056902)
XLA Ops:
  0.6 1.3 %broadcast_in_dim.31 = f32[1024]{0:T(1024)} convert(bf16[1024]{0:T(1024)(128)(2,1)} %param.57) | non-fusion elementwise | flops 1024 | bytes 6144 | tf_op jit(solution)/shard_map/broadcast_in_dim | solution.py:524
  1.9 8.9 %shard_map.308 = (bf16[8,1024]{1,0:T(8,128)(2,1)}, f32[8,16,64,128]{3,2,1,0:T(8,128)}, bf16[3,8,1024]{2,1,0:T(8,128)(2,1)}, bf16[3,8,512]{2,1,0:T(8,128)(2,1)}, bf16[3,8,512]{2,1,0:T(8,128)(2,1)}) custom-call(bf16[8,1024]{1,0:T(8,128)(2,1)} %tokens_ref.3, f32[1,1024]{1,0:T(1,128)} %bitcast.21, f32[8,16,64,128]{3,2,1,0:T(8,128)} %state_hbm.1, ...), custom_call_target="tpu_custom_call" | custom-call | flops 100000000 | bytes 14000000 | tf_op jit(solution)/shard_map/pallas_call | solution.py:177
  10.8 30.5 %shard_map.309 = bf16[8,512]{1,0:T(8,128)(2,1)} custom-call(bf16[8,1024]{1,0:T(8,128)(2,1)} %get-tuple-element.10.mixed_ref, bf16[1024,1024]{1,0:T(8,128)(2,1)} %w_out_hbm.1, bf16[8,1024]{1,0:T(8,128)(2,1)} %tokens_ref.3, f32[1,1024]{1,0:T(1,128)} %bitcast.23, s32[8,6]{1,0:T(8,128)} %ids_ref.1, f32[8,6]{1,0:T(8,128)} %weights_ref.1, ...), custom_call_target="tpu_custom_call" | custom-call | flops 1000000000 | bytes 10000000 | tf_op jit(solution)/shard_map/pallas_call | solution.py:479
  41.3 1.3 %copy.35 = bf16[8,512]{1,0:T(8,128)(2,1)} copy(bf16[8,512]{1,0:T(8,128)(2,1)} %shard_map.309) | data formatting | bytes 16384
